TPU v7x, 256 devices: a whole 4x4x8 slice. The times are simulated.
256 devices in a mesh: ep: 64 (over z, y, core), tp: 4 (over x).
Axes of the slice: x: 4, y: 4, z: 8, core: 2. Of those that a mesh axis runs over, the one named last changes fastest.
Arguments:
- mixer_input: bfloat16 [32768, 2048], P('ep'), may hold values from -6 to 6
- mixer_gain: bfloat16 [2048], replicated, may hold values from 0.099609375 to 1.8984375
- pool_in: bfloat16 [2048, 1024], P(None, 'tp'), may hold values from -0.125 to 0.125
- pool_map: bfloat16 [4, 256, 256], P('tp'), may hold values from -0.375 to 0.375
- pool_scale: bfloat16 [1024], P('tp'), may hold values from 0.099609375 to 1.8984375
- pool_out: bfloat16 [1024, 2048], P('tp'), may hold values from -0.1875 to 0.1875
- expert_input: bfloat16 [24576, 2048], P('ep'), may hold values from -6 to 6
- expert_gain: bfloat16 [2048], replicated, may hold values from 0.099609375 to 1.8984375
- group_router: bfloat16 [2048, 4], replicated, may hold values from -0.125 to 0.125
- expert_router: bfloat16 [2048, 64], replicated, may hold values from -0.125 to 0.125
- routes: int32 [24576, 2], P('ep'), may hold values from 0 to 63, all different within a row; in each aligned block of 96 rows (0 to 95, 96 to 191, ...) at most 6 rows name the same one
- gate_weight: bfloat16 [64, 2048, 1024], P('ep', None, 'tp'), may hold values from -0.125 to 0.125
- up_weight: bfloat16 [64, 2048, 1024], P('ep', None, 'tp'), may hold values from -0.125 to 0.125
- down_weight: bfloat16 [64, 1024, 2048], P('ep', 'tp'), may hold values from -0.1875 to 0.1875
Outputs:
- mixer_output: bfloat16 [32768, 2048], P(('ep', 'tp'))
- expert_output: bfloat16 [24576, 2048], P(('ep', 'tp'))
Inputs may be any that keep to these rules, and one draw needn't show every extreme that they name: `routes`: each row names two different experts. In each aligned block of 96 rows no expert is named more than 6 times, a bound that some block reaches.
All inputs are finite; a program needn't handle non-finite values.
Results may differ from a plain program's by a relative error of at most 0.01.
Values may be sent and summed in bfloat16 or wider, within the bound.
A program may use at most 64 MiB of HBM per device.

v0:
```python
import jax
import jax.numpy as jnp
from jax import lax
from jax.sharding import PartitionSpec as P

RIM = 15


EPS = 1e-06


def passed_along(value, axis, steps):
    count = lax.axis_size(axis)
    leading, last = (max(0, -steps), min(count, count - steps))
    return lax.ppermute(value, axis, [(source, source + steps) for source in range(leading, last)])


def norm_rows(values, gain):
    floats = values.astype(jnp.float32)
    scale = lax.rsqrt(jnp.mean(floats * floats, axis=-1, keepdims=True) + EPS)
    return (floats * scale * gain.astype(jnp.float32)).astype(jnp.bfloat16)


def route_weights(rows, group_router, expert_router, route_rows):
    group_logits = jnp.dot(rows, group_router, preferred_element_type=jnp.float32)
    expert_logits = jnp.dot(rows, expert_router, preferred_element_type=jnp.float32)
    groups = group_logits.shape[1]
    experts = expert_logits.shape[1]
    member = (
        jnp.arange(experts, dtype=jnp.int32)[:, None] // (experts // groups)
        == jnp.arange(groups, dtype=jnp.int32)[None, :]
    ).astype(jnp.float32)
    group_exp = jnp.exp(group_logits)
    group_prob = group_exp / jnp.sum(group_exp, axis=1, keepdims=True)
    expert_exp = jnp.exp(expert_logits)
    within = jnp.dot(expert_exp, member, precision=lax.Precision.HIGHEST)
    prob = expert_exp * jnp.dot(group_prob / within, member.T, precision=lax.Precision.HIGHEST)
    chosen = (route_rows[:, :, None] == jnp.arange(experts, dtype=jnp.int32)[None, None, :]).astype(
        jnp.float32
    )
    picked = jnp.sum(chosen * prob[:, None, :], axis=2)
    return picked / jnp.sum(picked, axis=1, keepdims=True)


def mixer_half(mixer_input, mixer_gain, pool_in, pool_map, pool_scale, pool_out):
    normed = norm_rows(mixer_input, mixer_gain)
    pooled_in = jnp.dot(normed, pool_in, preferred_element_type=jnp.float32).astype(jnp.bfloat16)
    local_rows = pooled_in.shape[0]
    groups_here = pool_map.shape[0]
    channels = pool_map.shape[1]
    border = passed_along(pooled_in[local_rows - RIM :], "ep", 1)
    padded = jnp.concatenate([border, pooled_in], axis=0).astype(jnp.float32)
    padded = padded.reshape(local_rows + RIM, groups_here, channels)
    leading = lax.axis_index("tp") * groups_here
    windows = jnp.left_shift(jnp.int32(2), leading + jnp.arange(groups_here, dtype=jnp.int32))
    window_sum = jnp.zeros((local_rows, groups_here, channels), jnp.float32)
    for offset in range(RIM + 1):
        active = (offset < windows).astype(jnp.float32)
        window_sum = (
            window_sum + padded[RIM - offset : RIM - offset + local_rows] * active[None, :, None]
        )
    position = lax.axis_index("ep") * local_rows + jnp.arange(local_rows, dtype=jnp.int32)
    counts_here = jnp.minimum(position[:, None] + 1, windows[None, :]).astype(jnp.float32)
    pooled = (window_sum / counts_here[:, :, None] - padded[RIM:]).astype(jnp.bfloat16)
    mapped = jnp.einsum("tgc,gce->tge", pooled, pool_map, preferred_element_type=jnp.float32)
    mixed_rows = (
        mapped.reshape(local_rows, groups_here * channels) * pool_scale.astype(jnp.float32)
    ).astype(jnp.bfloat16)
    return lax.psum_scatter(
        jnp.dot(mixed_rows, pool_out, preferred_element_type=jnp.float32).astype(jnp.bfloat16),
        "tp",
        scatter_dimension=0,
        tiled=True,
    )


def slot_positions(route_rows, blocks, experts):
    flat = route_rows.reshape(blocks, -1)
    onehot = (flat[:, :, None] == jnp.arange(experts, dtype=jnp.int32)[None, None, :]).astype(
        jnp.int32
    )
    before = jnp.cumsum(onehot, axis=1) - onehot
    return (jnp.sum(before * onehot, axis=2), flat)


def dispatch_rows(normed, route_rows, blocks, slots_each, experts):
    block_len = normed.shape[0] // blocks
    positions, flat = slot_positions(route_rows, blocks, experts)
    block_index = jnp.arange(blocks, dtype=jnp.int32)[:, None]
    slot_index = block_index * slots_each + positions
    token_index = block_index * block_len + jnp.arange(2 * block_len, dtype=jnp.int32)[None, :] // 2
    table = jnp.full((blocks * slots_each, experts), -1, jnp.int32)
    table = table.at[slot_index.reshape(-1), flat.reshape(-1)].set(token_index.reshape(-1))
    fetched = normed[jnp.maximum(table, 0)]
    return jnp.where((table >= 0)[:, :, None], fetched, jnp.zeros_like(fetched))


def expert_half(
    expert_input,
    expert_gain,
    group_router,
    expert_router,
    routes,
    gate_weight,
    up_weight,
    down_weight,
):
    normed = norm_rows(expert_input, expert_gain)
    tp_count = lax.axis_size("tp")
    tp_place = lax.axis_index("tp")
    experts = expert_router.shape[1]
    block_len = normed.shape[0] // tp_count
    slots_each = 4 * block_len // experts
    own_rows = lax.dynamic_slice_in_dim(normed, tp_place * block_len, block_len, 0)
    own_routes = lax.dynamic_slice_in_dim(routes, tp_place * block_len, block_len, 0)
    sending = dispatch_rows(own_rows, own_routes, 1, slots_each, experts)
    arrived = lax.all_to_all(sending, "ep", split_axis=1, concat_axis=1, tiled=True)
    received = lax.all_gather(arrived, "tp", axis=0, tiled=True)
    held = gate_weight.shape[0]
    model = received.shape[2]
    down_whole = lax.all_gather(down_weight, "tp", axis=1, tiled=True)
    all_slots = received.reshape(received.shape[0], -1, held, model)
    gate = jnp.einsum("csed,edh->cseh", all_slots, gate_weight, preferred_element_type=jnp.float32)
    upward = jnp.einsum("csed,edh->cseh", all_slots, up_weight, preferred_element_type=jnp.float32)
    hidden = (jax.nn.silu(gate) * upward).astype(jnp.bfloat16)
    swapped = lax.all_to_all(hidden, "tp", split_axis=0, concat_axis=3, tiled=True)
    hid_part = hidden.shape[3]
    total = jnp.zeros((swapped.shape[0], swapped.shape[1], held, model), jnp.float32)
    for part in range(tp_count):
        partial_value = jnp.einsum(
            "cseh,ehd->csed",
            swapped[:, :, :, part * hid_part : (part + 1) * hid_part],
            down_whole[:, part * hid_part : (part + 1) * hid_part],
            preferred_element_type=jnp.float32,
        ).astype(jnp.bfloat16)
        partial_value = lax.optimization_barrier(partial_value)
        total = total + partial_value.astype(jnp.float32)
    summed = total.astype(jnp.bfloat16).reshape(slots_each, -1, model)
    returned = lax.all_to_all(summed, "ep", split_axis=1, concat_axis=1, tiled=True)
    positions, flat = slot_positions(own_routes, 1, experts)
    lookup = positions[0] * experts + flat[0]
    picked = (
        returned.reshape(slots_each * experts, model)[lookup]
        .astype(jnp.float32)
        .reshape(block_len, 2, model)
    )
    weights = route_weights(own_rows, group_router, expert_router, own_routes)
    return jnp.sum(picked * weights[:, :, None], axis=1).astype(jnp.bfloat16)


def on_device(
    mixer_input,
    mixer_gain,
    pool_in,
    pool_map,
    pool_scale,
    pool_out,
    expert_input,
    expert_gain,
    group_router,
    expert_router,
    routes,
    gate_weight,
    up_weight,
    down_weight,
):
    mixer_output = mixer_half(mixer_input, mixer_gain, pool_in, pool_map, pool_scale, pool_out)
    expert_output = expert_half(
        expert_input,
        expert_gain,
        group_router,
        expert_router,
        routes,
        gate_weight,
        up_weight,
        down_weight,
    )
    return (mixer_output, expert_output)


def solution(mesh):
    return jax.shard_map(
        on_device,
        mesh=mesh,
        in_specs=(
            P("ep", None),
            P(),
            P(None, "tp"),
            P("tp", None, None),
            P("tp"),
            P("tp", None),
            P("ep", None),
            P(),
            P(),
            P(),
            P("ep", None),
            P("ep", None, "tp"),
            P("ep", None, "tp"),
            P("ep", "tp", None),
        ),
        out_specs=(P(("ep", "tp"), None), P(("ep", "tp"), None)),
        check_vma=False,
    )
```

profile of v0, /device:TPU:1, one launch (start us, length us, event | category | flops | bytes accessed | tf_op | source)
XLA Modules:
  0.0 302.3 jit_solution(5306408200580199578)
XLA Ops:
  7.2 0.0 copy-start
  7.2 0.0 all-gather.3.cloned.1.call-start
  7.2 0.9 constant_dynamic-slice_fusion
  8.2 0.1 copy.41
  8.3 0.1 eq.66
  8.4 0.1 fusion.51
  8.5 0.6 reduce-window.6
  9.1 0.2 slice_reduce_fusion
  9.3 0.1 copy.43
  9.4 0.1 reshape_reshape.3
  9.5 1.8 multiply_reduce_fusion
  11.3 2.0 convert_element_type.227
  13.4 0.1 copy.44
  13.5 0.1 broadcast.292
  13.7 0.1 add_bitcast_fusion
  13.7 0.1 fusion.52
  13.9 9.3 %scatter_fusion = s32[6,64]{1,0:T(8,128)S(1)} fusion(s32[6,64]{1,0:T(8,128)S(1)} %broadcast_in_dim.11, s32[192]{0:T(256)S(1)} %bitcast.129, s32[192]{0:T(256)S(1)} %and_select_fusion.1), kind=kCustom, calls=%fused_computation.2 | custom fusion | bytes 3840 | tf_op jit(solution)/shard_map/scatter | solution.py:93
  23.2 0.1 reshape.559
  23.3 0.1 dynamic-slice
  23.4 0.1 copy.46
  23.5 1.3 fusion.26
  24.8 2.5 gather_fusion
  27.2 1.0 copy_select_fusion
  28.2 62.6 %all_to_all.28 = bf16[6,64,2048]{2,0,1:T(8,128)(2,1)S(1)} all-to-all(bf16[6,64,2048]{2,0,1:T(8,128)(2,1)S(1)} %copy_select_fusion), channel_id=1, replica_groups=mesh['ep'=64,'tp'=4] {'ep'}, dimensions={1} | all-to-all | bytes 3145728 | tf_op jit(solution)/shard_map/all_to_all | solution.py:117
  90.9 2.0 copy.48
  92.9 0.0 all-gather.3.cloned.1.call-update
  92.9 0.0 all-gather.5.cloned.1.call-start
  93.0 0.7 all-gather.5.cloned.1.call-update
  93.7 0.8 copy-done.3
  94.5 0.5 fusion
  95.0 0.1 copy-done.11
  95.1 0.8 fusion.17
  95.9 0.7 copy-done.4
  96.6 5.1 %collective-permute-start = (bf16[15,256]{1,0:T(8,128)(2,1)S(1)}, bf16[15,256]{1,0:T(8,128)(2,1)S(1)}, u32[]{:S(2)}, u32[]{:S(2)}) collective-permute-start(bf16[15,256]{1,0:T(8,128)(2,1)S(1)} %slice.135), channel_id=1, source_target_pairs={{0,4},{4,8},{8,12},{12,16},{16,20},{20,24},{24,28},{28,32},{32,36}... | collective-permute-start | bytes 23048 | tf_op jit(solution)/shard_map/ppermute | solution.py:15
  101.7 56.9 %all-gather.3.cloned.1.call-done = bf16[24,64,2048]{2,1,0:T(8,128)(2,1)} async-done(((bf16[6,64,2048]{2,1,0:T(8,128)(2,1)}), bf16[24,64,2048]{2,1,0:T(8,128)(2,1)}) %all-gather.3.cloned.1.call-update) | async-done | bytes 6291472 | tf_op jit(solution)/shard_map/all_gather | solution.py:118
  158.7 5.1 %fusion.23 = f32[24,64,256]{2,1,0:T(8,128)S(1)} fusion(bf16[24,64,2048]{2,1,0:T(8,128)(2,1)} %all-gather.3.cloned.1.call-done, bf16[1,2048,256]{2,1,0:T(8,128)(2,1)} %param.25), kind=kOutput, calls=%fused_computation.46 | convolution fusion | flops 1610612736 | bytes 8912896 | tf_op jit(solution)/shard_map/csed,edh->cseh/dot_general | solution.py:123
  163.7 0.1 copy-done.12
  163.8 3.0 fusion.16
  166.8 3.6 %all-to-all-start.1 = ((bf16[24,64,1,256]{3,1,2,0:T(8,128)(2,1)}), bf16[24,64,1,256]{3,1,2,0:T(8,128)(2,1)S(1)}, u32[]{:S(2)}, u32[]{:S(2)}) async-start(bf16[24,64,1,256]{3,1,2,0:T(8,128)(2,1)} %fusion.16), calls=%async_computation.2 | async-start | bytes 1572864 | tf_op jit(solution)/shard_map/all_to_all | solution.py:126
  170.4 0.2 reduce-scatter.2.cloned.1.call-start
  170.7 0.1 maximum_convert_fusion
  170.8 3.3 %convolution_convert_fusion = bf16[512,2048]{1,0:T(8,128)(2,1)} fusion(bf16[256,2048]{1,0:T(8,128)(2,1)S(1)} %copy-done, f32[256]{0:T(256)S(1)} %convert_element_type.223, f32[527,256]{1,0:T(8,128)S(1)} %maximum_convert_fusion, f32[512]{0:T(512)S(1)} %minimum_convert_fusion, f32[]{:T(128)S(6)} %convert_element_type.220, f32[]{:T(128)S(6)} %convert_element_type.219, ...), kind=kOutput, calls=%fused_computation.10 | convolution fusion | flops 609746944 | bytes 11668544 | tf_op jit(solution)/shard_map/dot_general | solution.py:70
  174.1 0.0 reduce-scatter.2.cloned.1.call-update
  174.1 10.8 %all-to-all-done.1 = bf16[24,64,1,256]{3,1,2,0:T(8,128)(2,1)S(1)} async-done(((bf16[24,64,1,256]{3,1,2,0:T(8,128)(2,1)}), bf16[24,64,1,256]{3,1,2,0:T(8,128)(2,1)S(1)}, u32[]{:S(2)}, u32[]{:S(2)}) %all-to-all-start.1) | async-done | bytes 786464 | tf_op jit(solution)/shard_map/all_to_all | solution.py:126
  184.9 0.6 copy.56
  185.5 0.6 all_to_all.23
  186.1 30.8 %all-gather.5.cloned.1.call-done = bf16[1,1024,2048]{2,1,0:T(8,128)(2,1)} async-done(((bf16[1,256,2048]{2,1,0:T(8,128)(2,1)}), bf16[1,1024,2048]{2,1,0:T(8,128)(2,1)}) %all-gather.5.cloned.1.call-update) | async-done | bytes 4194320 | tf_op jit(solution)/shard_map/all_gather | solution.py:121
  216.9 2.0 fusion.3
  218.9 1.8 fusion.4
  220.7 0.6 fusion.5
  221.3 0.6 fusion.6
  221.9 1.4 fusion.11
  223.2 2.2 copy.51
  225.4 10.9 %all-to-all-start.2 = ((bf16[6,64,2048]{2,0,1:T(8,128)(2,1)}), bf16[6,64,2048]{2,0,1:T(8,128)(2,1)}, u32[]{:S(2)}, u32[]{:S(2)}) async-start(bf16[6,64,2048]{2,0,1:T(8,128)(2,1)} %copy.51), calls=%async_computation.3 | async-start | bytes 4194304 | tf_op jit(solution)/shard_map/all_to_all | solution.py:139
  236.4 0.2 fusion.56
  236.6 0.3 convolution_exponential_fusion
  236.9 0.2 fusion.21
  237.1 0.2 convolution_multiply_fusion.1
  237.4 0.1 copy.53
  237.5 48.4 %all-to-all-done.2 = bf16[6,64,2048]{2,0,1:T(8,128)(2,1)} async-done(((bf16[6,64,2048]{2,0,1:T(8,128)(2,1)}), bf16[6,64,2048]{2,0,1:T(8,128)(2,1)}, u32[]{:S(2)}, u32[]{:S(2)}) %all-to-all-start.2) | async-done | bytes 1572896 | tf_op jit(solution)/shard_map/all_to_all | solution.py:139
  285.9 2.5 copy.52
  288.4 2.1 gather_fusion.1
  290.5 2.1 reshape.556
  292.6 3.1 %multiply_reduce_fusion.1 = bf16[96,2048]{1,0:T(8,128)(2,1)} fusion(f32[96,2,2048]{2,1,0:T(2,128)S(1)} %reshape.556, f32[96,2]{1,0:T(8,128)S(1)} %copy.53), kind=kLoop, calls=%fused_computation.31 | loop fusion | flops 589824 | bytes 1966848 | tf_op jit(solution)/shard_map/reduce_sum | solution.py:148
  (48 shorter events, 0.3 us)
Async XLA Ops:
  7.2 163.6 %copy-start = (bf16[256,2048]{1,0:T(8,128)(2,1)S(1)}, bf16[256,2048]{1,0:T(8,128)(2,1)}, u32[]{:S(2)}) copy-start(bf16[256,2048]{1,0:T(8,128)(2,1)} %param.19) | copy-start | bytes 3145732
  7.2 4.2 %copy-start.1 = (bf16[384,2048]{1,0:T(8,128)(2,1)S(1)}, bf16[384,2048]{1,0:T(8,128)(2,1)}, u32[]{:S(2)}) copy-start(bf16[384,2048]{1,0:T(8,128)(2,1)} %param.20) | copy-start | bytes 4718596
  7.2 151.5 %all-gather.3.cloned.1.call-start = ((), (), s32[]{:S(2)}) async-start(), calls=%async_computation.5 | async-start | bytes 7864320 | tf_op jit(solution)/shard_map/all_gather | solution.py:118
  13.4 10.0 %copy-start.8 = (bf16[2048]{0:T(1024)(128)(2,1)S(1)}, bf16[2048]{0:T(1024)(128)(2,1)}, u32[]{:S(2)}) copy-start(bf16[2048]{0:T(1024)(128)(2,1)} %param.21) | copy-start | bytes 12292
  92.9 0.8 copy-start.9
  92.9 1.6 copy-start.3
  92.9 124.0 %all-gather.5.cloned.1.call-start = ((), (), s32[]{:S(2)}) async-start(), calls=%async_computation.6 | async-start | bytes 5242880 | tf_op jit(solution)/shard_map/all_gather | solution.py:121
  93.7 1.4 copy-start.11
  95.1 6.6 %copy-start.14 = (bf16[256]{0:T(256)(128)(2,1)S(1)}, bf16[256]{0:T(256)(128)(2,1)}, u32[]{:S(2)}) copy-start(bf16[256]{0:T(256)(128)(2,1)} %param.18) | copy-start | bytes 1540
  95.9 0.7 copy-start.4
  96.6 74.1 %collective-permute-start = (bf16[15,256]{1,0:T(8,128)(2,1)S(1)}, bf16[15,256]{1,0:T(8,128)(2,1)S(1)}, u32[]{:S(2)}, u32[]{:S(2)}) collective-permute-start(bf16[15,256]{1,0:T(8,128)(2,1)S(1)} %slice.135), channel_id=1, source_target_pairs={{0,4},{4,8},{8,12},{12,16},{16,20},{20,24},{24,28},{28,32},{32,36}... | collective-permute-start | bytes 23048 | tf_op jit(solution)/shard_map/ppermute | solution.py:15
  158.7 5.1 %copy-start.10 = (bf16[24,64,2048]{2,1,0:T(8,128)(2,1)S(1)}, bf16[24,64,2048]{2,1,0:T(8,128)(2,1)}, u32[]{:S(2)}) copy-start(bf16[24,64,2048]{2,1,0:T(8,128)(2,1)} %all-gather.3.cloned.1.call-done) | copy-start | bytes 18874372
  158.7 5.1 %copy-start.12 = (bf16[1,2048,256]{2,1,0:T(8,128)(2,1)S(1)}, bf16[1,2048,256]{2,1,0:T(8,128)(2,1)}, u32[]{:S(2)}) copy-start(bf16[1,2048,256]{2,1,0:T(8,128)(2,1)} %param.26) | copy-start | bytes 3145732
  163.8 6.9 %copy-start.5 = (bf16[512,256]{1,0:T(8,128)(2,1)S(1)}, bf16[512,256]{1,0:T(8,128)(2,1)}, u32[]{:S(2)}) copy-start(bf16[512,256]{1,0:T(8,128)(2,1)} %copy-done.4) | copy-start | bytes 786436
  166.8 4.0 %copy-start.13 = (bf16[1,256,256]{2,1,0:T(8,128)(2,1)S(1)}, bf16[1,256,256]{2,1,0:T(8,128)(2,1)}, u32[]{:S(2)}) copy-start(bf16[1,256,256]{2,1,0:T(8,128)(2,1)} %param.17) | copy-start | bytes 393220
  166.8 18.1 %all-to-all-start.1 = ((bf16[24,64,1,256]{3,1,2,0:T(8,128)(2,1)}), bf16[24,64,1,256]{3,1,2,0:T(8,128)(2,1)S(1)}, u32[]{:S(2)}, u32[]{:S(2)}) async-start(bf16[24,64,1,256]{3,1,2,0:T(8,128)(2,1)} %fusion.16), calls=%async_computation.2 | async-start | bytes 1572864 | tf_op jit(solution)/shard_map/all_to_all | solution.py:126
  170.4 125.3 %reduce-scatter.2.cloned.1.call-start = ((), (), s32[]{:S(2)}) async-start(), calls=%async_computation.4 | async-start | bytes 2621440 | tf_op jit(solution)/shard_map/reduce_scatter | solution.py:69
  216.9 3.8 %copy-start.2 = (bf16[1,1024,2048]{2,1,0:T(8,128)(2,1)S(1)}, bf16[1,1024,2048]{2,1,0:T(8,128)(2,1)}, u32[]{:S(2)}) copy-start(bf16[1,1024,2048]{2,1,0:T(8,128)(2,1)} %all-gather.5.cloned.1.call-done) | copy-start | bytes 12582916
  225.4 10.9 %copy-start.7 = (bf16[2048,4]{0,1:T(4,128)(2,1)S(1)}, bf16[2048,4]{0,1:T(4,128)(2,1)}, u32[]{:S(2)}) copy-start(bf16[2048,4]{0,1:T(4,128)(2,1)} %param.22) | copy-start | bytes 49156
  225.4 11.1 %copy-start.6 = (bf16[2048,64]{0,1:T(8,128)(2,1)S(1)}, bf16[2048,64]{0,1:T(8,128)(2,1)}, u32[]{:S(2)}) copy-start(bf16[2048,64]{0,1:T(8,128)(2,1)} %param.23) | copy-start | bytes 786436
  225.4 60.5 %all-to-all-start.2 = ((bf16[6,64,2048]{2,0,1:T(8,128)(2,1)}), bf16[6,64,2048]{2,0,1:T(8,128)(2,1)}, u32[]{:S(2)}, u32[]{:S(2)}) async-start(bf16[6,64,2048]{2,0,1:T(8,128)(2,1)} %copy.51), calls=%async_computation.3 | async-start | bytes 4194304 | tf_op jit(solution)/shard_map/all_to_all | solution.py:139
Sparse Core Ops, SparseCore 0:
  93.0 65.5 all-gather.2
  160.5 56.3 all-gather.4
  220.0 31.7 reduce-scatter.1
where the time goes:
time: 303 us; the launch traced here: 302 us
  waiting for transfers between devices  148 us (49%)
  blocking collectives  62.6 us (21%)
  local copies, waits for them, and re-layouts  27.7 us (9%)
  starting transfers between devices  19.9 us (7%)
  matrix products  18 us (6%)
  between operations  14.2 us (5%)
  other arithmetic  12.1 us (4%)
    all_to_all x1, blocking collectives, expert_half(): lax.all_to_all(sending, 'ep', split_axis=1, concat_axis=1, tiled=True)  62.6 us
    all_gather x1, waiting for transfers between devices, expert_half(): received = lax.all_gather(arrived, 'tp', axis=0, tiled=True)  56.9 us
    all_to_all x1, waiting for transfers between devices, expert_half(): lax.all_to_all(summed, 'ep', split_axis=1, concat_axis=1, tiled=True)  48.4 us
    all_gather x1, waiting for transfers between devices, expert_half(): down_whole = lax.all_gather(down_weight, 'tp', axis=1, tiled=True)  30.8 us
    all_to_all x1, starting transfers between devices, expert_half(): lax.all_to_all(summed, 'ep', split_axis=1, concat_axis=1, tiled=True)  10.9 us
    all_to_all x1, waiting for transfers between devices, expert_half(): lax.all_to_all(hidden, 'tp', split_axis=0, concat_axis=3, tiled=True)  10.8 us
    scatter x1, local copies, waits for them, and re-layouts, dispatch_rows(): table.at[slot_index.reshape(-1), flat.reshape(-1)]  9.28 us
  transfers between devices with their start and end apart: 6, of which 4 were waited for; matrix products, arithmetic and copies ran while one was open for 11% of the time, Pallas kernels for 0%

commit v1 on v0

v1 whole, which is shorter than its diff:
```python
import functools

import jax
import jax.numpy as jnp
from jax import lax
from jax.experimental import pallas as pl
from jax.experimental.pallas import tpu as pltpu
from jax.sharding import PartitionSpec as P

EPS = 1e-06
RIM = 16
CHUNKS = 4
MESH = pl.DeviceIdType.MESH
F32 = jnp.float32
BF16 = jnp.bfloat16


def iota(shape, dim):
    return lax.broadcasted_iota(jnp.int32, shape, dim)


def over(value, divisor):
    return (value * (-(-65536 // divisor))) >> 16


def ones_where(mask):
    return jnp.where(mask, 1.0, 0.0).astype(BF16)


def dot(a, b):
    return jnp.dot(a, b, preferred_element_type=F32)


def norm_rows(values, gain):
    floats = values.astype(F32)
    scale = lax.rsqrt(jnp.mean(floats * floats, axis=-1, keepdims=True) + EPS)
    return (floats * scale * gain.astype(F32)).astype(BF16)


def kernel(
    n,
    cap,
    mix_hbm,
    mix_gain,
    pool_in_hbm,
    pool_map,
    pool_scale,
    pool_out_hbm,
    exp_hbm,
    exp_gain,
    group_router,
    expert_router,
    routes,
    gate_hbm,
    up_hbm,
    down_hbm,
    mix_out,
    exp_out,
    mix_in,
    pool_in,
    pool_out,
    pin,
    border,
    mixed,
    mpart,
    mrecv1,
    msend2,
    mrecv2,
    xin,
    normed,
    perm,
    pick,
    ysend,
    ybuf,
    zsend,
    rows,
    gate,
    up,
    down,
    gsum,
    usum,
    hidden,
    psend,
    precv,
    pown,
    zsend2,
    zbuf2,
    ysend2,
    ybuf2,
    local_sem,
    ys,
    yr,
    zs,
    zr,
    ys2,
    yr2,
    zs2,
    zr2,
    rs,
    rr,
    ps,
    pr,
    ws,
    wr,
    ms,
    mr,
):
    ep, tp = lax.axis_index("ep"), lax.axis_index("tp")
    z, yc = ep // n, ep % n
    devices = n * n
    mate = tp + 1 - 2 * (tp % 2)
    across = 3 - tp
    ahead, behind = (ep + 1) % devices, (ep + devices - 1) % devices
    tokens, model = xin.shape
    experts = expert_router.shape[1]
    slots = ysend.shape[0]
    block = slots // n
    width = model // CHUNKS
    hid = gate.shape[2]

    def cols(k):
        return pl.ds(pl.multiple_of(k * width, width), width)

    def part(index):
        return pl.ds(pl.multiple_of(index * block, 16), block)

    def remote(src, dst, send, recv, ep_to, tp_to):
        return pltpu.make_async_remote_copy(
            src_ref=src,
            dst_ref=dst,
            send_sem=send,
            recv_sem=recv,
            device_id={"ep": ep_to, "tp": tp_to},
            device_id_type=MESH,
        )

    local = [
        pltpu.make_async_copy(
            exp_hbm.at[pl.ds(pl.multiple_of(tp * tokens, 16), tokens)], xin, local_sem.at[0]
        ),
        pltpu.make_async_copy(mix_hbm, mix_in, local_sem.at[1]),
        pltpu.make_async_copy(pool_in_hbm, pool_in, local_sem.at[2]),
        pltpu.make_async_copy(pool_out_hbm, pool_out, local_sem.at[3]),
        pltpu.make_async_copy(gate_hbm.at[0], gate.at[0], local_sem.at[4]),
        pltpu.make_async_copy(up_hbm.at[0], up.at[0], local_sem.at[5]),
        pltpu.make_async_copy(down_hbm.at[0], down.at[0], local_sem.at[6]),
    ]
    for copy in local:
        copy.start()

    barrier = pltpu.get_barrier_semaphore()

    def greet(ep_to, tp_to):
        pl.semaphore_signal(
            barrier, inc=1, device_id={"ep": ep_to, "tp": tp_to}, device_id_type=MESH
        )

    @pl.loop(1, n)
    def _(d):
        greet(((z + d) % n) * n + yc, tp)
        greet(z * n + (yc + d) % n, tp)

    greet(ep, mate)
    greet(ep, across)
    greet(ahead, tp)
    greet(behind, tp)
    pl.semaphore_wait(barrier, 2 * (n - 1) + 4)

    def gate_copy(k):
        return remote(
            gate_hbm.at[0, cols(k)], gate.at[1, cols(k)], ws.at[0, k], wr.at[0, k], ep, mate
        )

    def up_copy(k):
        return remote(up_hbm.at[0, cols(k)], up.at[1, cols(k)], ws.at[1, k], wr.at[1, k], ep, mate)

    def down_copy(k):
        return remote(
            down_hbm.at[0, :, cols(k)],
            down.at[1, :, cols(k)],
            ws.at[2, k],
            wr.at[2, k],
            ep,
            mate,
        )

    @pl.loop(0, CHUNKS)
    def _(k):
        gate_copy(k).start()
        up_copy(k).start()

    @pl.loop(0, CHUNKS)
    def _(k):
        down_copy(k).start()

    def y_copy(src, dst, send, recv, k, d):
        to = (yc + d) % n
        return remote(
            src.at[part(to), cols(k)],
            dst.at[part(yc), cols(k)],
            send.at[k, d],
            recv.at[k, d],
            z * n + to,
            tp,
        )

    def z_copy(src, dst, send, recv, k, d):
        to = (z + d) % n
        return remote(
            src.at[part(to), cols(k)],
            dst.at[part(z), cols(k)],
            send.at[k, d],
            recv.at[k, d],
            to * n + yc,
            tp,
        )

    def start_all(copy, *args):
        @pl.loop(1, n)
        def _(d):
            copy(*args, d).start()

    def recv_all(copy, *args):
        @pl.loop(1, n)
        def _(d):
            copy(*args, d).wait_recv()

    def sent_all(copy, *args):
        @pl.loop(1, n)
        def _(d):
            copy(*args, d).wait_send()

    y_out = (y_copy, ysend, ybuf, ys, yr)
    z_out = (z_copy, zsend, rows.at[0], zs, zr)
    z_back = (z_copy, zsend2, zbuf2, zs2, zr2)
    y_back = (y_copy, ysend2, ybuf2, ys2, yr2)

    local[0].wait()
    normed[...] = norm_rows(xin[...], exp_gain[...])
    named = routes[pl.ds(pl.multiple_of(tp * tokens, 16), tokens), :]
    first, second = named[:, 0:1], named[:, 1:2]
    lanes = iota((tokens, experts), 1)
    routed = jnp.where((first == lanes) | (second == lanes), 1.0, 0.0)
    earlier = ones_where(iota((tokens, tokens), 1) < iota((tokens, tokens), 0))
    rank = dot(earlier, routed.astype(BF16))

    def slot_of(shape, dim):
        c = iota(shape, dim)
        y = over(c, n * cap)
        inner = c - y * (n * cap)
        zz = over(inner, cap)
        return zz * n + y, inner - zz * cap

    expert_c, place_c = slot_of((experts, slots), 1)
    spread = ones_where(iota((experts, slots), 0) == expert_c)
    ranks = dot((routed * (rank + 1.0)).astype(BF16), spread)
    expert_t, place_t = slot_of((tokens, slots), 1)
    chosen = jnp.where(ranks == (place_t + 1).astype(F32), 1.0, 0.0)
    pick[pl.ds(0, tokens), :] = jnp.where(first == expert_t, chosen, 0.0).astype(BF16)
    pick[pl.ds(tokens, tokens), :] = jnp.where(second == expert_t, chosen, 0.0).astype(BF16)
    chosen = chosen.astype(BF16)

    for k in range(CHUNKS):
        ysend[:, cols(k)] = lax.dot_general(
            chosen, normed[:, cols(k)], (((0,), (0,)), ((), ())), preferred_element_type=F32
        ).astype(BF16)
        start_all(*y_out, k)
        ybuf[part(yc), cols(k)] = ysend[part(yc), cols(k)]

    o = iota((slots, slots), 0)
    oa = over(o, block)
    ob = over(o - oa * block, cap)
    perm[...] = ones_where(iota((slots, slots), 1) == ob * block + oa * cap + (o - oa * block - ob * cap))

    def to_z(k):
        recv_all(*y_out, k)
        zsend[:, cols(k)] = dot(perm[...], ybuf[:, cols(k)]).astype(BF16)
        start_all(*z_out, k)
        rows[0, part(z), cols(k)] = zsend[part(z), cols(k)]

    local[1].wait()
    local[2].wait()
    total = mix_in.shape[0]
    step = 128

    @pl.loop(0, total // step)
    def _(b):
        at = pl.multiple_of(b * step, step)
        good = norm_rows(mix_in[pl.ds(at, step), :], mix_gain[...])
        pin[pl.ds(at + step, step), :] = dot(good, pool_in[...]).astype(BF16)

    border_copy = remote(
        pin.at[pl.ds(total + step - RIM, RIM)], border, ms.at[0], mr.at[0], ahead, tp
    )
    border_copy.start()

    to_z(0)

    border_copy.wait_recv()
    pin[pl.ds(0, step - RIM), :] = jnp.zeros((step - RIM, pin.shape[1]), BF16)
    edge = border[...].astype(F32)
    pin[pl.ds(step - RIM, RIM), :] = jnp.where(ep == 0, jnp.zeros_like(edge), edge).astype(BF16)
    window = jnp.left_shift(jnp.int32(2), tp)
    back = iota((step, 2 * step), 0) + step - iota((step, 2 * step), 1)
    band = ones_where((back >= 0) & (back < window))
    local[3].wait()

    @pl.loop(0, total // step)
    def _(b):
        at = pl.multiple_of(b * step, step)
        window_sum = dot(band, pin[pl.ds(at, 2 * step), :])
        position = ep * total + at + iota((step, 1), 0)
        count = jnp.minimum(position + 1, window).astype(F32)
        own = pin[pl.ds(at + step, step), :].astype(F32)
        pooled = (window_sum / count - own).astype(BF16)
        mixed[pl.ds(at, step), :] = (
            dot(pooled, pool_map[0]) * pool_scale[...].astype(F32)
        ).astype(BF16)

    to_z(1)

    half = total // 2
    quarter = total // 4
    away = pl.multiple_of((1 - tp // 2) * half, half)
    kept = pl.multiple_of((tp // 2) * half, half)

    def mix_project(start):
        @pl.loop(0, 2)
        def _(b):
            at = pl.multiple_of(start + b * quarter, quarter)
            mpart[pl.ds(at, quarter), :] = dot(mixed[pl.ds(at, quarter), :], pool_out[...]).astype(BF16)

    mix_project(away)
    mix_copy1 = remote(mpart.at[pl.ds(away, half)], mrecv1, ms.at[1], mr.at[1], ep, across)
    mix_copy1.start()
    to_z(2)
    mix_project(kept)
    to_z(3)

    gsum[...] = jnp.zeros_like(gsum)
    usum[...] = jnp.zeros_like(usum)
    for copy in local[4:]:
        copy.wait()

    def row_copy(k):
        return remote(rows.at[0, :, cols(k)], rows.at[1, :, cols(k)], rs.at[k], rr.at[k], ep, across)

    def accumulate(r, w, k):
        x = rows[r, :, cols(k)]
        gsum[r, w] += dot(x, gate[w, cols(k), :])
        usum[r, w] += dot(x, up[w, cols(k), :])

    @pl.loop(0, CHUNKS)
    def _(k):
        recv_all(*z_out, k)
        row_copy(k).start()
        accumulate(0, 0, k)

    mix_copy1.wait_recv()
    theirs = pl.multiple_of((mate % 2) * quarter, quarter)
    mine = pl.multiple_of((tp % 2) * quarter, quarter)
    msend2[...] = (
        mpart[pl.ds(kept + theirs, quarter), :].astype(F32)
        + mrecv1[pl.ds(theirs, quarter), :].astype(F32)
    ).astype(BF16)
    mix_copy2 = remote(msend2, mrecv2, ms.at[2], mr.at[2], ep, mate)
    mix_copy2.start()

    @pl.loop(0, CHUNKS)
    def _(k):
        gate_copy(k).wait_recv()
        up_copy(k).wait_recv()
        accumulate(0, 1, k)

    @pl.loop(0, CHUNKS)
    def _(k):
        row_copy(k).wait_recv()
        accumulate(1, 0, k)
        accumulate(1, 1, k)

    @pl.loop(0, 2)
    def _(r):
        @pl.loop(0, 2)
        def _(w):
            g = gsum[r, w]
            hidden[r, w] = (jax.nn.silu(g) * usum[r, w]).astype(BF16)

    def partial_copy(k):
        return remote(psend.at[:, cols(k)], precv.at[:, cols(k)], ps.at[k], pr.at[k], ep, across)

    def project(r, k):
        return dot(hidden[r, 0], down[0, :, cols(k)]) + dot(hidden[r, 1], down[1, :, cols(k)])

    def down_stage(k):
        down_copy(k).wait_recv()
        psend[:, cols(k)] = project(1, k).astype(BF16)
        partial_copy(k).start()
        pown[:, cols(k)] = project(0, k)

    def z_stage(k):
        partial_copy(k).wait_recv()
        zsend2[:, cols(k)] = (pown[:, cols(k)] + precv[:, cols(k)].astype(F32)).astype(BF16)
        start_all(*z_back, k)
        zbuf2[part(z), cols(k)] = zsend2[part(z), cols(k)]

    def y_stage(k):
        recv_all(*z_back, k)
        ysend2[:, cols(k)] = dot(perm[...], zbuf2[:, cols(k)]).astype(BF16)
        start_all(*y_back, k)
        ybuf2[part(yc), cols(k)] = ysend2[part(yc), cols(k)]

    own_rows = normed[...]
    group_exp = jnp.exp(dot(own_rows, group_router[...]))
    group_prob = group_exp / jnp.sum(group_exp, axis=1, keepdims=True)
    expert_exp = jnp.exp(dot(own_rows, expert_router[...]))
    groups = group_exp.shape[1]
    ratio = jnp.zeros_like(expert_exp)
    for q in range(groups):
        inside = over(lanes, experts // groups) == q
        within = jnp.sum(jnp.where(inside, expert_exp, 0.0), axis=1, keepdims=True)
        ratio = ratio + jnp.where(inside, group_prob[:, q : q + 1] / within, 0.0)
    prob = expert_exp * ratio
    picked0 = jnp.sum(jnp.where(first == lanes, prob, 0.0), axis=1, keepdims=True)
    picked1 = jnp.sum(jnp.where(second == lanes, prob, 0.0), axis=1, keepdims=True)
    weight0 = picked0 / (picked0 + picked1)
    weight1 = picked1 / (picked0 + picked1)

    def finish(k):
        recv_all(*y_back, k)
        both = dot(pick[...], ybuf2[:, cols(k)])
        exp_out[:, cols(k)] = (weight0 * both[:tokens] + weight1 * both[tokens:]).astype(BF16)

    stages = (down_stage, z_stage, y_stage, finish)
    for turn in range(CHUNKS + len(stages) - 1):
        for s, stage in enumerate(stages):
            if 0 <= turn - s < CHUNKS:
                stage(turn - s)

    mix_copy2.wait_recv()
    mix_out[...] = (
        mpart[pl.ds(kept + mine, quarter), :].astype(F32)
        + mrecv1[pl.ds(mine, quarter), :].astype(F32)
        + mrecv2[...].astype(F32)
    ).astype(BF16)

    border_copy.wait_send()
    mix_copy1.wait_send()
    mix_copy2.wait_send()

    @pl.loop(0, CHUNKS)
    def _(k):
        gate_copy(k).wait_send()
        up_copy(k).wait_send()
        down_copy(k).wait_send()
        row_copy(k).wait_send()
        partial_copy(k).wait_send()
        sent_all(*y_out, k)
        sent_all(*z_out, k)
        sent_all(*z_back, k)
        sent_all(*y_back, k)


def on_device(n, *args):
    (
        mixer_input,
        mixer_gain,
        pool_in,
        pool_map,
        pool_scale,
        pool_out,
        expert_input,
        expert_gain,
        group_router,
        expert_router,
        routes,
        gate_weight,
        up_weight,
        down_weight,
    ) = args
    total, model = mixer_input.shape
    channels = pool_in.shape[1]
    tokens = expert_input.shape[0] // 4
    experts = expert_router.shape[1]
    cap = 4 * tokens // experts
    slots = cap * experts
    hid = gate_weight.shape[2]
    vmem = pl.BlockSpec(memory_space=pltpu.VMEM)
    hbm = pl.BlockSpec(memory_space=pl.ANY)
    dma = pltpu.SemaphoreType.DMA
    each = dma((CHUNKS, n))
    return pl.pallas_call(
        functools.partial(kernel, n, cap),
        out_shape=(
            jax.ShapeDtypeStruct((total // 4, model), BF16),
            jax.ShapeDtypeStruct((tokens, model), BF16),
        ),
        in_specs=[hbm, vmem, hbm, vmem, vmem, hbm, hbm, vmem, vmem, vmem, vmem, hbm, hbm, hbm],
        out_specs=(vmem, vmem),
        scratch_shapes=[
            pltpu.VMEM((total, model), BF16),
            pltpu.VMEM((model, channels), BF16),
            pltpu.VMEM((channels, model), BF16),
            pltpu.VMEM((total + 128, channels), BF16),
            pltpu.VMEM((RIM, channels), BF16),
            pltpu.VMEM((total, channels), BF16),
            pltpu.VMEM((total, model), BF16),
            pltpu.VMEM((total // 2, model), BF16),
            pltpu.VMEM((total // 4, model), BF16),
            pltpu.VMEM((total // 4, model), BF16),
            pltpu.VMEM((tokens, model), BF16),
            pltpu.VMEM((tokens, model), BF16),
            pltpu.VMEM((slots, slots), BF16),
            pltpu.VMEM((2 * tokens, slots), BF16),
            pltpu.VMEM((slots, model), BF16),
            pltpu.VMEM((slots, model), BF16),
            pltpu.VMEM((slots, model), BF16),
            pltpu.VMEM((2, slots, model), BF16),
            pltpu.VMEM((2, model, hid), BF16),
            pltpu.VMEM((2, model, hid), BF16),
            pltpu.VMEM((2, hid, model), BF16),
            pltpu.VMEM((2, 2, slots, hid), F32),
            pltpu.VMEM((2, 2, slots, hid), F32),
            pltpu.VMEM((2, 2, slots, hid), BF16),
            pltpu.VMEM((slots, model), BF16),
            pltpu.VMEM((slots, model), BF16),
            pltpu.VMEM((slots, model), F32),
            pltpu.VMEM((slots, model), BF16),
            pltpu.VMEM((slots, model), BF16),
            pltpu.VMEM((slots, model), BF16),
            pltpu.VMEM((slots, model), BF16),
            dma((7,)),
            each,
            each,
            each,
            each,
            each,
            each,
            each,
            each,
            dma((CHUNKS,)),
            dma((CHUNKS,)),
            dma((CHUNKS,)),
            dma((CHUNKS,)),
            dma((3, CHUNKS)),
            dma((3, CHUNKS)),
            dma((3,)),
            dma((3,)),
        ],
        compiler_params=pltpu.CompilerParams(
            collective_id=0, has_side_effects=True, vmem_limit_bytes=60 * 1024 * 1024
        ),
    )(
        mixer_input,
        mixer_gain.reshape(1, model),
        pool_in,
        pool_map,
        pool_scale.reshape(1, channels),
        pool_out,
        expert_input,
        expert_gain.reshape(1, model),
        group_router,
        expert_router,
        routes,
        gate_weight,
        up_weight,
        down_weight,
    )


def solution(mesh):
    n = 1
    while n * n < mesh.shape["ep"]:
        n += 1
    return jax.shard_map(
        functools.partial(on_device, n),
        mesh=mesh,
        in_specs=(
            P("ep", None),
            P(),
            P(None, "tp"),
            P("tp", None, None),
            P("tp"),
            P("tp", None),
            P("ep", None),
            P(),
            P(),
            P(),
            P("ep", None),
            P("ep", None, "tp"),
            P("ep", None, "tp"),
            P("ep", "tp", None),
        ),
        out_specs=(P(("ep", "tp"), None), P(("ep", "tp"), None)),
        check_vma=False,
    )
```

time: 303 us -> 157 us (0.52)
  waiting for transfers between devices: 148 us -> 0 us
  Pallas kernels: 0 us -> 141 us
  blocking collectives: 62.6 us -> 0 us
  starting transfers between devices: 19.9 us -> 0 us
  matrix products: 18 us -> 0 us
  local copies, waits for them, and re-layouts: 27.7 us -> 12.7 us
  between operations: 14.2 us -> 0.64 us
  other arithmetic: 12.1 us -> 0 us
    pallas_call x0 -> x1, Pallas kernels: none -> 141 us  [on_device(): pl.pallas_call(functools.partial(kernel, n, cap), out_shape=(jax.ShapeDty...]
    all_gather x2 -> x0, waiting for transfers between devices: 87.7 us -> none  [the longest x1 56.9 us: expert_half(): received = lax.all_gather(arrived, 'tp', axis=0, tiled=True)]
    all_to_all x1 -> x0, blocking collectives: 62.6 us -> none  [expert_half(): lax.all_to_all(sending, 'ep', split_axis=1, concat_axis=1, tiled=True)]
    all_to_all x2 -> x0, waiting for transfers between devices: 59.2 us -> none  [the longest x1 48.4 us: expert_half(): lax.all_to_all(summed, 'ep', split_axis=1, concat_axis=1, tiled=True)]
    dot_general x12 -> x0, matrix products: 18 us -> none  [the longest x1 5.05 us: expert_half(): jnp.einsum('csed,edh->cseh', all_slots, gate_weight, preferred_element_ty...]
    all_to_all x2 -> x0, starting transfers between devices: 14.5 us -> none  [the longest x1 10.9 us: expert_half(): lax.all_to_all(summed, 'ep', split_axis=1, concat_axis=1, tiled=True)]
    scatter x1 -> x0, local copies, waits for them, and re-layouts: 9.28 us -> none  [dispatch_rows(): table.at[slot_index.reshape(-1), flat.reshape(-1)]]
    unnamed x30 -> x5, local copies, waits for them, and re-layouts: 1.7 us -> 8.86 us
  transfers between devices with their start and end apart: 6 -> 0, of which waited for: 4 -> 0; matrix products, arithmetic and copies ran while one was open for 11% -> 0% of each run, Pallas kernels for 0% -> 0%
where the time goes in v1:
time: 157 us; the launch traced here: 155 us
  Pallas kernels  141 us (90%)
  local copies, waits for them, and re-layouts  12.7 us (8%)
    pallas_call x1, Pallas kernels, on_device(): pl.pallas_call(functools.partial(kernel, n, cap), out_shape=(jax.ShapeDty...  141 us
    unnamed x5, local copies, waits for them, and re-layouts  8.86 us

profile of v1, /device:TPU:1, one launch (start us, length us, event | category | flops | bytes accessed | tf_op | source)
XLA Modules:
  0.0 154.6 jit_solution(5136354819422152140)
XLA Ops:
  0.6 1.2 reshape.14.pool_scale
  1.9 1.3 reshape.13.mix_gain
  3.1 1.3 reshape.15.exp_gain
  4.4 1.5 copy.18.routes
  5.9 1.8 %copy.16.group_router = bf16[2048,4]{1,0:T(8,128)(2,1)} copy(bf16[2048,4]{0,1:T(4,128)(2,1)} %param.22) | data formatting | bytes 32768 | tf_op args[8]
  7.7 1.9 %copy.17.expert_router = bf16[2048,64]{1,0:T(8,128)(2,1)} copy(bf16[2048,64]{0,1:T(8,128)(2,1)} %param.23) | data formatting | bytes 524288 | tf_op args[9]
  9.6 141.3 %shard_map.149 = (bf16[128,2048]{1,0:T(8,128)(2,1)}, bf16[96,2048]{1,0:T(8,128)(2,1)}) custom-call(bf16[512,2048]{1,0:T(8,128)(2,1)} %mix_hbm.1, bf16[1,2048]{1,0:T(2,128)(2,1)} %reshape.13.mix_gain, bf16[2048,256]{1,0:T(8,128)(2,1)} %pool_in_hbm.1, bf16[1,256,256]{2,1,0:T(8,128)(2,1)} %pool_map.1, bf16[1,256]{1,0:T(2,128)(2,1)} %reshape.14.pool_scale, ...), custom_call_target="tpu_custom_call" | custom-call | tf_op jit(solution)/shard_map/pallas_call | solution.py:491
  150.9 1.9 %copy.21 = bf16[128,2048]{1,0:T(8,128)(2,1)} copy(bf16[128,2048]{1,0:T(8,128)(2,1)} %get-tuple-element.4) | data formatting | bytes 1048576
  152.8 1.8 %copy.22 = bf16[96,2048]{1,0:T(8,128)(2,1)} copy(bf16[96,2048]{1,0:T(8,128)(2,1)} %get-tuple-element.5) | data formatting | bytes 786432

commit v2 on v1

v2 whole, which is shorter than its diff:
```python
import functools

import jax
import jax.numpy as jnp
from jax import lax
from jax.experimental import pallas as pl
from jax.experimental.pallas import tpu as pltpu
from jax.sharding import PartitionSpec as P

EPS = 1e-06
RIM = 16
CHUNKS = 8
Z_FIRST = 2
PIECES = 4
ACROSS_FIRST = 1
BACK = (256,) * 7 + (128, 128)
scope = jax.named_scope
MESH = pl.DeviceIdType.MESH
F32 = jnp.float32
BF16 = jnp.bfloat16


def iota(shape, dim):
    return lax.broadcasted_iota(jnp.int32, shape, dim)


def over(value, divisor):
    return (value * (-(-65536 // divisor))) >> 16


def ones_where(mask):
    return jnp.where(mask, 1.0, 0.0).astype(BF16)


def dot(a, b):
    return jnp.dot(a, b, preferred_element_type=F32)


def dot_t(a, b):
    return lax.dot_general(a, b, (((1,), (1,)), ((), ())), preferred_element_type=F32)


def norm_rows(values, gain):
    floats = values.astype(F32)
    scale = lax.rsqrt(jnp.mean(floats * floats, axis=-1, keepdims=True) + EPS)
    return (floats * scale * gain.astype(F32)[None, :]).astype(BF16)


def kernel(
    n,
    cap,
    mix_hbm,
    mix_gain,
    pool_in_hbm,
    pool_map,
    pool_scale,
    pool_out_hbm,
    exp_hbm,
    exp_gain,
    group_router,
    expert_router,
    routes,
    gate_hbm,
    up_hbm,
    down_hbm,
    mix_out,
    exp_out,
    mix_in,
    pool_in,
    pool_out,
    pin,
    border,
    mixed,
    mpart,
    mrecv1,
    msend2,
    mrecv2,
    xin,
    normed,
    perm,
    pick,
    ysend,
    ybuf,
    zsend,
    rows,
    gate,
    up,
    down,
    gsum,
    usum,
    hidden,
    psend,
    precv,
    pown,
    zsend2,
    zbuf2,
    ysend2,
    ybuf2,
    local_sem,
    ys,
    yr,
    zs,
    zr,
    ys2,
    yr2,
    zs2,
    zr2,
    rs,
    rr,
    ps,
    pr,
    ws,
    wr,
    ms,
    mr,
    mix1s,
    mix1r,
    mix2s,
    mix2r,
    yland,
    exp_fin,
    mix_fin,
    exp_sem,
    mix_sem,
):
    ep, tp = lax.axis_index("ep"), lax.axis_index("tp")
    z, yc = ep // n, ep % n
    devices = n * n
    mate = tp + 1 - 2 * (tp % 2)
    across = 3 - tp
    ahead, behind = (ep + 1) % devices, (ep + devices - 1) % devices
    tokens, model = xin.shape
    experts = expert_router.shape[0]
    slots = ysend.shape[0]
    block = slots // n
    width = model // CHUNKS
    hid = gate.shape[2]

    def cols(k):
        return pl.ds(pl.multiple_of(k * width, width), width)

    def part(index):
        return pl.ds(pl.multiple_of(index * block, 16), block)

    def remote(src, dst, send, recv, ep_to, tp_to):
        return pltpu.make_async_remote_copy(
            src_ref=src,
            dst_ref=dst,
            send_sem=send,
            recv_sem=recv,
            device_id={"ep": ep_to, "tp": tp_to},
            device_id_type=MESH,
        )

    local = [
        pltpu.make_async_copy(
            exp_hbm.at[pl.ds(pl.multiple_of(tp * tokens, 16), tokens)], xin, local_sem.at[0]
        ),
        pltpu.make_async_copy(mix_hbm, mix_in, local_sem.at[1]),
        pltpu.make_async_copy(pool_in_hbm, pool_in, local_sem.at[2]),
        pltpu.make_async_copy(pool_out_hbm, pool_out, local_sem.at[3]),
        pltpu.make_async_copy(gate_hbm.at[0], gate.at[0], local_sem.at[4]),
        pltpu.make_async_copy(up_hbm.at[0], up.at[0], local_sem.at[5]),
        pltpu.make_async_copy(down_hbm.at[0], down.at[0], local_sem.at[6]),
    ]
    for copy in local:
        copy.start()

    barrier = pltpu.get_barrier_semaphore()

    def greet(ep_to, tp_to):
        pl.semaphore_signal(
            barrier, inc=1, device_id={"ep": ep_to, "tp": tp_to}, device_id_type=MESH
        )

    @pl.loop(1, n)
    def _(d):
        greet(((z + d) % n) * n + yc, tp)
        greet(z * n + (yc + d) % n, tp)

    greet(ep, mate)
    greet(ep, across)
    greet(ahead, tp)
    greet(behind, tp)
    def gate_copy(k):
        return remote(
            gate_hbm.at[0, cols(k)], gate.at[1, cols(k)], ws.at[0, k], wr.at[0, k], ep, mate
        )

    def up_copy(k):
        return remote(up_hbm.at[0, cols(k)], up.at[1, cols(k)], ws.at[1, k], wr.at[1, k], ep, mate)

    def down_copy(k):
        return remote(
            down_hbm.at[0, :, cols(k)],
            down.at[1, :, cols(k)],
            ws.at[2, k],
            wr.at[2, k],
            ep,
            mate,
        )

    def y_copy(src, dst, send, recv, k, at, d):
        to = (yc + d) % n
        return remote(src.at[part(to), at], dst.at[part(yc), at], send, recv.at[k], z * n + to, tp)

    def z_copy(src, dst, send, recv, k, at, d):
        to = (z + d) % n
        return remote(src.at[part(to), at], dst.at[part(z), at], send, recv.at[k], to * n + yc, tp)

    def start_all(copy, *args):
        @pl.loop(1, n)
        def _(d):
            copy(*args, d).start()

    others = pl.ds(0, slots - block)

    def recv_all(copy, src, dst, send, recv, k, at):
        remote(src.at[others, at], dst.at[others, at], send, recv.at[k], ep, mate).wait_recv()

    def sent_all(src, send):
        remote(src.at[others], src.at[others], send, zr.at[0], ep, mate).wait_send()

    y_out = (y_copy, ysend, ybuf, ys, yr)
    z_out = (z_copy, zsend, rows.at[0], zs, zr)
    z_early = (z_copy, zsend, ybuf, zs, zr)
    y_late = (y_copy, ysend, yland, ys, yr)
    z_back = (z_copy, zsend2, zbuf2, zs2, zr2)
    y_back = (y_copy, ysend2, ybuf2, ys2, yr2)

    local[0].wait()
    normed[...] = norm_rows(xin[...], exp_gain[...])
    everyone = routes.shape[1]
    named = routes[...].astype(F32)
    here = iota((tokens, everyone), 1) == tp * tokens + iota((tokens, everyone), 0)
    first, second = [
        jnp.sum(jnp.where(here, named[j : j + 1, :], 0.0), axis=1, keepdims=True).astype(jnp.int32)
        for j in range(2)
    ]
    here = iota((everyone, tokens), 0) == tp * tokens + iota((everyone, tokens), 1)
    named = dot(named.astype(BF16), ones_where(here)).astype(jnp.int32)
    lanes = iota((experts, tokens), 0)
    routed = jnp.where((named[0:1, :] == lanes) | (named[1:2, :] == lanes), 1.0, 0.0)
    earlier = ones_where(iota((tokens, tokens), 0) < iota((tokens, tokens), 1))
    rank = (routed * (dot(routed.astype(BF16), earlier) + 1.0)).astype(BF16)

    def slot_of(shape, dim):
        c = iota(shape, dim)
        outer = over(c, n * cap)
        inner = over(c - outer * (n * cap), cap)
        return outer, inner, c - outer * (n * cap) - inner * cap

    def packing(z_major):
        outer, inner, _ = slot_of((slots, experts), 0)
        expert = outer * n + inner if z_major else inner * n + outer
        ranks = dot(ones_where(iota((slots, experts), 1) == expert), rank)
        return ones_where(ranks == (slot_of((slots, tokens), 0)[2] + 1).astype(F32))

    early = pl.ds(0, Z_FIRST * width)
    late = pl.ds(Z_FIRST * width, model - Z_FIRST * width)
    zsend[:, early] = dot(packing(True), normed[:, early]).astype(BF16)
    ysend[:, late] = dot(packing(False), normed[:, late]).astype(BF16)

    local[1].wait()
    local[2].wait()
    total = mix_in.shape[0]
    step = 128

    @pl.loop(0, total // step)
    def _(b):
        at = pl.multiple_of(b * step, step)
        good = norm_rows(mix_in[pl.ds(at, step), :], mix_gain[...])
        pin[pl.ds(at + step, step), :] = dot(good, pool_in[...]).astype(BF16)

    border_copy = remote(
        pin.at[pl.ds(total + step - RIM, RIM)], border, ms.at[0], mr.at[0], ahead, tp
    )

    with scope("barrier"):
        pl.semaphore_wait(barrier, 2 * (n - 1) + 4)
    border_copy.start()

    for k in range(Z_FIRST):
        start_all(*z_early, k, cols(k))
    for k in range(Z_FIRST, Z_FIRST + 3):
        start_all(*y_out, k, cols(k))

    @pl.loop(0, CHUNKS)
    def _(k):
        gate_copy(k).start()
        up_copy(k).start()

    @pl.loop(0, CHUNKS)
    def _(k):
        down_copy(k).start()

    ybuf[part(z), early] = zsend[part(z), early]
    ybuf[part(yc), late] = ysend[part(yc), late]

    outer, inner, place = slot_of((slots, slots), 0)
    perm[...] = ones_where(iota((slots, slots), 1) == inner * block + outer * cap + place)

    def to_y(k):
        with scope("wait_z"):
            recv_all(*z_early, k, cols(k))
        ysend[:, cols(k)] = dot(perm[...], ybuf[:, cols(k)]).astype(BF16)
        start_all(*y_late, k, cols(k))
        yland[part(yc), cols(k)] = ysend[part(yc), cols(k)]

    def to_z(k):
        with scope("wait_y"):
            recv_all(*y_out, k, cols(k))
        zsend[:, cols(k)] = dot(perm[...], ybuf[:, cols(k)]).astype(BF16)
        start_all(*z_out, k, cols(k))
        rows[0, part(z), cols(k)] = zsend[part(z), cols(k)]
        part_copy(k, 0).start()

    def part_copy(k, d):
        at = part((z + d) % n)
        return remote(
            rows.at[0, at, cols(k)], rows.at[1, at, cols(k)], rs.at[k], rr.at[k], ep, across
        )

    def row_copy(k):
        return remote(rows.at[0, :, cols(k)], rows.at[1, :, cols(k)], rs.at[k], rr.at[k], ep, across)

    def arrive_late(k):
        with scope("wait_y"):
            recv_all(*y_late, k, cols(k))
        rows[0, :, cols(k)] = dot(perm[...], yland[:, cols(k)]).astype(BF16)
        row_copy(k).start()

    def arrive(k):
        with scope("wait_z"):
            recv_all(*z_out, k, cols(k))

        @pl.loop(1, n)
        def _(d):
            part_copy(k, d).start()


    with scope("wait_border"):
        border_copy.wait_recv()
    pin[pl.ds(0, step - RIM), :] = jnp.zeros((step - RIM, pin.shape[1]), BF16)
    edge = border[...].astype(F32)
    pin[pl.ds(step - RIM, RIM), :] = jnp.where(ep == 0, jnp.zeros_like(edge), edge).astype(BF16)
    window = jnp.left_shift(jnp.int32(2), tp)
    back = iota((step, 2 * step), 0) + step - iota((step, 2 * step), 1)
    band = ones_where((back >= 0) & (back < window))
    local[3].wait()

    @pl.loop(0, total // step)
    def _(b):
        at = pl.multiple_of(b * step, step)
        window_sum = dot(band, pin[pl.ds(at, 2 * step), :])
        position = ep * total + at + iota((step, 1), 0)
        count = jnp.minimum(position + 1, window).astype(F32)
        own = pin[pl.ds(at + step, step), :].astype(F32)
        pooled = (window_sum / count - own).astype(BF16)
        mixed[pl.ds(at, step), :] = (
            dot(pooled, pool_map[0]) * pool_scale[...].astype(F32)[None, :]
        ).astype(BF16)

    quarter = total // 4
    wide = model // PIECES

    def quarter_rows(index):
        return pl.ds(pl.multiple_of(index * quarter, quarter), quarter)

    def piece(j):
        return pl.ds(j * wide, wide)

    def steps(j):
        return (across, mate) if j < ACROSS_FIRST else (mate, across)

    def mix_copy1(j, s):
        return remote(
            mpart.at[quarter_rows(3 - mate if s else steps(j)[0]), piece(j)],
            mrecv1.at[s, :, piece(j)],
            mix1s.at[j, s],
            mix1r.at[j, s],
            ep,
            steps(j)[0],
        )

    def mix_copy2(j):
        return remote(
            msend2.at[:, piece(j)], mrecv2.at[:, piece(j)], mix2s.at[j], mix2r.at[j], ep, steps(j)[1]
        )

    def mix_project(j):
        mpart[:, piece(j)] = dot(mixed[...], pool_out[:, piece(j)]).astype(BF16)
        mix_copy1(j, 0).start()
        mix_copy1(j, 1).start()

    def mix_stage(j):
        with scope("wait_mix1"):
            mix_copy1(j, 0).wait_recv()
            mix_copy1(j, 1).wait_recv()
        msend2[:, piece(j)] = (
            mpart[quarter_rows(steps(j)[1]), piece(j)].astype(F32)
            + mrecv1[1, :, piece(j)].astype(F32)
        ).astype(BF16)
        mix_copy2(j).start()

    def mix_out_copy(j):
        return pltpu.make_async_copy(
            mix_fin.at[:, piece(j)], mix_out.at[:, piece(j)], mix_sem.at[j]
        )

    def mix_finish(j):
        with scope("wait_mix2"):
            mix_copy2(j).wait_recv()
        mix_fin[:, piece(j)] = (
            mpart[quarter_rows(tp), piece(j)].astype(F32)
            + mrecv1[0, :, piece(j)].astype(F32)
            + mrecv2[:, piece(j)].astype(F32)
        ).astype(BF16)
        mix_out_copy(j).start()

    for j in range(ACROSS_FIRST):
        mix_project(j)
    to_z(Z_FIRST)
    to_z(Z_FIRST + 1)
    to_y(0)
    start_all(*y_out, Z_FIRST + 3, cols(Z_FIRST + 3))
    to_z(Z_FIRST + 2)
    for j in range(ACROSS_FIRST, PIECES):
        mix_project(j)
    to_y(1)
    for k in range(Z_FIRST + 4, CHUNKS):
        start_all(*y_out, k, cols(k))
    arrive_late(0)
    to_z(Z_FIRST + 3)
    arrive_late(1)
    to_z(Z_FIRST + 4)
    arrive(Z_FIRST)
    to_z(Z_FIRST + 5)

    gsum[...] = jnp.zeros_like(gsum)
    usum[...] = jnp.zeros_like(usum)
    for copy in local[4:]:
        copy.wait()

    def accumulate(r, w, k):
        x = rows[r, :, cols(k)]
        gsum[r, w] += dot(x, gate[w, cols(k), :])
        usum[r, w] += dot(x, up[w, cols(k), :])

    @pl.loop(0, Z_FIRST + 1)
    def _(k):
        accumulate(0, 0, k)

    @pl.loop(Z_FIRST + 1, CHUNKS)
    def _(k):
        arrive(k)
        accumulate(0, 0, k)

    for j in range(ACROSS_FIRST):
        mix_stage(j)

    lanes = iota((tokens, experts), 1)
    routed = jnp.where((first == lanes) | (second == lanes), 1.0, 0.0)
    earlier = ones_where(iota((tokens, tokens), 1) < iota((tokens, tokens), 0))
    rank = (routed * (dot(earlier, routed.astype(BF16)) + 1.0)).astype(BF16)
    outer, inner, _ = slot_of((experts, slots), 1)
    ranks = dot(rank, ones_where(iota((experts, slots), 0) == inner * n + outer))
    outer, inner, place = slot_of((tokens, slots), 1)
    expert = inner * n + outer
    chosen = ranks == (place + 1).astype(F32)
    pick[pl.ds(0, tokens), :] = ones_where(chosen & (first == expert))
    pick[pl.ds(tokens, tokens), :] = ones_where(chosen & (second == expert))
    own_rows = normed[...]
    group_exp = jnp.exp(dot_t(own_rows, group_router[...]))
    group_prob = group_exp / jnp.sum(group_exp, axis=1, keepdims=True)
    expert_exp = jnp.exp(dot_t(own_rows, expert_router[...]))
    groups = group_exp.shape[1]
    ratio = jnp.zeros_like(expert_exp)
    for q in range(groups):
        inside = over(lanes, experts // groups) == q
        within = jnp.sum(jnp.where(inside, expert_exp, 0.0), axis=1, keepdims=True)
        ratio = ratio + jnp.where(inside, group_prob[:, q : q + 1] / within, 0.0)
    prob = expert_exp * ratio
    picked0 = jnp.sum(jnp.where(first == lanes, prob, 0.0), axis=1, keepdims=True)
    picked1 = jnp.sum(jnp.where(second == lanes, prob, 0.0), axis=1, keepdims=True)
    weight0 = picked0 / (picked0 + picked1)
    weight1 = picked1 / (picked0 + picked1)

    @pl.loop(0, CHUNKS)
    def _(k):
        with scope("wait_w"):
            gate_copy(k).wait_recv()
            up_copy(k).wait_recv()
        accumulate(0, 1, k)
        with scope("wait_r"):
            row_copy(k).wait_recv()
        accumulate(1, 0, k)
        accumulate(1, 1, k)

    @pl.loop(0, 2)
    def _(r):
        @pl.loop(0, 2)
        def _(w):
            g = gsum[r, w]
            hidden[r, w] = (jax.nn.silu(g) * usum[r, w]).astype(BF16)

    spans = [pl.ds(sum(BACK[:k]), BACK[k]) for k in range(len(BACK))]

    def partial_copy(k):
        at = spans[k]
        return remote(psend.at[:, at], precv.at[:, at], ps.at[k], pr.at[k], ep, across)

    def project(r, at):
        return dot(hidden[r, 0], down[0, :, at]) + dot(hidden[r, 1], down[1, :, at])

    def down_stage(k):
        at = spans[k]
        if at.start % width == 0:
            with scope("wait_down"):
                down_copy(at.start // width).wait_recv()
        psend[:, at] = project(1, at).astype(BF16)
        partial_copy(k).start()
        pown[:, at] = project(0, at)

    def z_stage(k):
        at = spans[k]
        with scope("wait_part"):
            partial_copy(k).wait_recv()
        zsend2[:, at] = (pown[:, at] + precv[:, at].astype(F32)).astype(BF16)
        start_all(*z_back, k, at)
        zbuf2[part(z), at] = zsend2[part(z), at]

    def y_stage(k):
        at = spans[k]
        with scope("wait_zb"):
            recv_all(*z_back, k, at)
        ysend2[:, at] = dot(perm[...], zbuf2[:, at]).astype(BF16)
        start_all(*y_back, k, at)
        ybuf2[part(yc), at] = ysend2[part(yc), at]

    def exp_copy(k):
        at = spans[k]
        return pltpu.make_async_copy(exp_fin.at[:, at], exp_out.at[:, at], exp_sem.at[k])

    def finish(k):
        at = spans[k]
        with scope("wait_yb"):
            recv_all(*y_back, k, at)
        both = dot(pick[...], ybuf2[:, at])
        exp_fin[:, at] = (weight0 * both[:tokens] + weight1 * both[tokens:]).astype(BF16)
        exp_copy(k).start()

    stages = ((down_stage, 0), (z_stage, 2), (y_stage, 4), (finish, 6))
    for turn in range(len(BACK) + 6):
        for stage, later in stages:
            if 0 <= turn - later < len(BACK):
                with scope(stage.__name__):
                    stage(turn - later)
        if 0 <= turn - len(BACK) + 1 < PIECES - ACROSS_FIRST:
            mix_stage(turn - len(BACK) + 1 + ACROSS_FIRST)
    for j in range(PIECES):
        mix_finish(j)

    with scope("sent"):
        border_copy.wait_send()
        for src, send in ((ysend, ys), (zsend, zs), (ysend2, ys2), (zsend2, zs2)):
            sent_all(src, send)

    for j in range(PIECES):
        mix_copy1(j, 0).wait_send()
        mix_copy1(j, 1).wait_send()
        mix_copy2(j).wait_send()

    @pl.loop(0, CHUNKS)
    def _(k):
        gate_copy(k).wait_send()
        up_copy(k).wait_send()
        down_copy(k).wait_send()
        row_copy(k).wait_send()

    for k in range(len(BACK)):
        partial_copy(k).wait_send()
        exp_copy(k).wait()

    for j in range(PIECES):
        mix_out_copy(j).wait()


def write_out(mix_from, exp_from, mix_to, exp_to, mix_held, exp_held, in_sem, out_sem):
    whole = ((mix_from, mix_held, mix_to), (exp_from, exp_held, exp_to))

    def copies(i, h):
        source, held, target = whole[i]
        size = held.shape[0] // 2
        at = pl.ds(h * size, size)
        return (
            pltpu.make_async_copy(source.at[at], held.at[at], in_sem.at[i, h]),
            pltpu.make_async_copy(held.at[at], target.at[at], out_sem.at[i, h]),
        )

    each = [copies(i, h) for i in range(2) for h in range(2)]
    for copy_in, _ in each:
        copy_in.start()
    for copy_in, copy_out in each:
        copy_in.wait()
        copy_out.start()
    for _, copy_out in each:
        copy_out.wait()


def on_device(n, *args):
    (
        mixer_input,
        mixer_gain,
        pool_in,
        pool_map,
        pool_scale,
        pool_out,
        expert_input,
        expert_gain,
        group_router,
        expert_router,
        routes,
        gate_weight,
        up_weight,
        down_weight,
    ) = args
    total, model = mixer_input.shape
    channels = pool_in.shape[1]
    tokens = expert_input.shape[0] // 4
    experts = expert_router.shape[1]
    cap = 4 * tokens // experts
    slots = cap * experts
    hid = gate_weight.shape[2]
    vmem = pl.BlockSpec(memory_space=pltpu.VMEM)
    hbm = pl.BlockSpec(memory_space=pl.ANY)
    dma = pltpu.SemaphoreType.DMA
    each, back = dma((CHUNKS,)), dma((len(BACK),))
    sent = pl.pallas_call(
        functools.partial(kernel, n, cap),
        out_shape=(
            jax.ShapeDtypeStruct((total // 4, model), BF16),
            jax.ShapeDtypeStruct((tokens, model), BF16),
        ),
        in_specs=[hbm, vmem, hbm, vmem, vmem, hbm, hbm, vmem, vmem, vmem, vmem, hbm, hbm, hbm],
        out_specs=(hbm, hbm),
        scratch_shapes=[
            pltpu.VMEM((total, model), BF16),
            pltpu.VMEM((model, channels), BF16),
            pltpu.VMEM((channels, model), BF16),
            pltpu.VMEM((total + 128, channels), BF16),
            pltpu.VMEM((RIM, channels), BF16),
            pltpu.VMEM((total, channels), BF16),
            pltpu.VMEM((total, model), BF16),
            pltpu.VMEM((2, total // 4, model), BF16),
            pltpu.VMEM((total // 4, model), BF16),
            pltpu.VMEM((total // 4, model), BF16),
            pltpu.VMEM((tokens, model), BF16),
            pltpu.VMEM((tokens, model), BF16),
            pltpu.VMEM((slots, slots), BF16),
            pltpu.VMEM((2 * tokens, slots), BF16),
            pltpu.VMEM((slots, model), BF16),
            pltpu.VMEM((slots, model), BF16),
            pltpu.VMEM((slots, model), BF16),
            pltpu.VMEM((2, slots, model), BF16),
            pltpu.VMEM((2, model, hid), BF16),
            pltpu.VMEM((2, model, hid), BF16),
            pltpu.VMEM((2, hid, model), BF16),
            pltpu.VMEM((2, 2, slots, hid), F32),
            pltpu.VMEM((2, 2, slots, hid), F32),
            pltpu.VMEM((2, 2, slots, hid), BF16),
            pltpu.VMEM((slots, model), BF16),
            pltpu.VMEM((slots, model), BF16),
            pltpu.VMEM((slots, model), F32),
            pltpu.VMEM((slots, model), BF16),
            pltpu.VMEM((slots, model), BF16),
            pltpu.VMEM((slots, model), BF16),
            pltpu.VMEM((slots, model), BF16),
            dma((7,)),
            dma,
            each,
            dma,
            each,
            dma,
            back,
            dma,
            back,
            each,
            each,
            back,
            back,
            dma((3, CHUNKS)),
            dma((3, CHUNKS)),
            dma((1,)),
            dma((1,)),
            dma((PIECES, 2)),
            dma((PIECES, 2)),
            dma((PIECES,)),
            dma((PIECES,)),
            pltpu.VMEM((slots, Z_FIRST * model // CHUNKS), BF16),
            pltpu.VMEM((tokens, model), BF16),
            pltpu.VMEM((total // 4, model), BF16),
            dma((len(BACK),)),
            dma((PIECES,)),
        ],
        compiler_params=pltpu.CompilerParams(
            collective_id=0, has_side_effects=True, vmem_limit_bytes=60 * 1024 * 1024
        ),
    )(
        mixer_input,
        mixer_gain,
        pool_in,
        pool_map,
        pool_scale,
        pool_out,
        expert_input,
        expert_gain,
        group_router.T,
        expert_router.T,
        routes.T,
        gate_weight,
        up_weight,
        down_weight,
    )
    shapes = [(total // 4, model), (tokens, model)]
    return pl.pallas_call(
        write_out,
        out_shape=tuple(jax.ShapeDtypeStruct(shape, BF16) for shape in shapes),
        in_specs=[hbm, hbm],
        out_specs=(hbm, hbm),
        scratch_shapes=[pltpu.VMEM(shape, BF16) for shape in shapes] + [dma((2, 2)), dma((2, 2))],
        cost_estimate=pl.CostEstimate(flops=0, bytes_accessed=4 * 224 * model, transcendentals=0),
    )(*sent)


def solution(mesh):
    n = 1
    while n * n < mesh.shape["ep"]:
        n += 1
    return jax.shard_map(
        functools.partial(on_device, n),
        mesh=mesh,
        in_specs=(
            P("ep", None),
            P(),
            P(None, "tp"),
            P("tp", None, None),
            P("tp"),
            P("tp", None),
            P("ep", None),
            P(),
            P(),
            P(),
            P("ep", None),
            P("ep", None, "tp"),
            P("ep", None, "tp"),
            P("ep", "tp", None),
        ),
        out_specs=(P(("ep", "tp"), None), P(("ep", "tp"), None)),
        check_vma=False,
    )
```

time: 157 us -> 117 us (0.75); the launches traced: 155 us -> 117 us
  Pallas kernels: 141 us -> 116 us
  local copies, waits for them, and re-layouts: 12.7 us -> 0 us
    pallas_call x1, Pallas kernels: 141 us -> 114 us  [on_device(): pl.pallas_call(functools.partial(kernel, n, cap), out_shape=(jax.ShapeDty...]
    unnamed x5 -> x0, local copies, waits for them, and re-layouts: 8.86 us -> none
    reshape x3 -> x0, local copies, waits for them, and re-layouts: 3.8 us -> none  [the longest x1 1.29 us: on_device(): expert_gain.reshape(1, model)]
    pallas_call x0 -> x1, Pallas kernels: none -> 1.93 us  [on_device(): pl.pallas_call(write_out, out_shape=tuple((jax.ShapeDtypeStruct(shape, BF...]
where the time goes in v2:
time: 117 us
  Pallas kernels  116 us (99%)
    pallas_call x1, Pallas kernels, on_device(): pl.pallas_call(functools.partial(kernel, n, cap), out_shape=(jax.ShapeDty...  114 us

profile of v2, /device:TPU:1, one launch (start us, length us, event | category | flops | bytes accessed | tf_op | source)
XLA Modules:
  0.0 116.8 jit_solution(2566720737595975458)
XLA Ops:
  0.6 114.2 %shard_map.149 = (bf16[128,2048]{1,0:T(8,128)(2,1)}, bf16[96,2048]{1,0:T(8,128)(2,1)}) custom-call(bf16[512,2048]{1,0:T(8,128)(2,1)} %mix_hbm.1, bf16[2048]{0:T(1024)(128)(2,1)} %mix_gain.1, bf16[2048,256]{1,0:T(8,128)(2,1)} %pool_in_hbm.1, bf16[1,256,256]{2,1,0:T(8,128)(2,1)} %pool_map.1, bf16[256]{0:T(256)(128)(2,1)} %pool_scale.1, ...), custom_call_target="tpu_custom_call" | custom-call | tf_op jit(solution)/shard_map/pallas_call | solution.py:639
  114.9 1.9 %shard_map.150 = (bf16[128,2048]{1,0:T(8,128)(2,1)}, bf16[96,2048]{1,0:T(8,128)(2,1)}) custom-call(bf16[128,2048]{1,0:T(8,128)(2,1)} %get-tuple-element.4.mix_from, bf16[96,2048]{1,0:T(8,128)(2,1)} %get-tuple-element.5.exp_from), custom_call_target="tpu_custom_call" | custom-call | bytes 1835008 | tf_op jit(solution)/shard_map/pallas_call | solution.py:726

commit v3 on v2

--- a/solution.py
+++ b/solution.py
@@ -13,7 +13,7 @@
 Z_FIRST = 2
 PIECES = 4
 ACROSS_FIRST = 1
-BACK = (256,) * 7 + (128, 128)
+BACK = (128, 128) + (256,) * 6 + (128, 128)
 scope = jax.named_scope
 MESH = pl.DeviceIdType.MESH
 F32 = jnp.float32
@@ -50,16 +50,16 @@
     n,
     cap,
     mix_hbm,
-    mix_gain,
+    mix_gain_hbm,
     pool_in_hbm,
-    pool_map,
-    pool_scale,
+    pool_map_hbm,
+    pool_scale_hbm,
     pool_out_hbm,
     exp_hbm,
-    exp_gain,
-    group_router,
-    expert_router,
-    routes,
+    exp_gain_hbm,
+    group_router_hbm,
+    expert_router_hbm,
+    routes_hbm,
     gate_hbm,
     up_hbm,
     down_hbm,
@@ -122,6 +122,15 @@
     mix_fin,
     exp_sem,
     mix_sem,
+    ds,
+    dr,
+    mix_gain,
+    pool_map,
+    pool_scale,
+    exp_gain,
+    group_router,
+    expert_router,
+    routes,
 ):
     ep, tp = lax.axis_index("ep"), lax.axis_index("tp")
     z, yc = ep // n, ep % n
@@ -152,6 +161,22 @@
             device_id_type=MESH,
         )
 
+    barrier = pltpu.get_barrier_semaphore()
+
+    def greet(ep_to, tp_to):
+        pl.semaphore_signal(
+            barrier, inc=1, device_id={"ep": ep_to, "tp": tp_to}, device_id_type=MESH
+        )
+
+    @pl.loop(1, n)
+    def _(d):
+        greet(((z + d) % n) * n + yc, tp)
+        greet(z * n + (yc + d) % n, tp)
+
+    greet(ep, mate)
+    greet(ep, across)
+    greet(ahead, tp)
+    greet(behind, tp)
     local = [
         pltpu.make_async_copy(
             exp_hbm.at[pl.ds(pl.multiple_of(tp * tokens, 16), tokens)], xin, local_sem.at[0]
@@ -162,26 +187,19 @@
         pltpu.make_async_copy(gate_hbm.at[0], gate.at[0], local_sem.at[4]),
         pltpu.make_async_copy(up_hbm.at[0], up.at[0], local_sem.at[5]),
         pltpu.make_async_copy(down_hbm.at[0], down.at[0], local_sem.at[6]),
+        pltpu.make_async_copy(exp_gain_hbm, exp_gain, local_sem.at[7]),
+        pltpu.make_async_copy(routes_hbm, routes, local_sem.at[8]),
+        pltpu.make_async_copy(mix_gain_hbm, mix_gain, local_sem.at[9]),
+        pltpu.make_async_copy(pool_map_hbm, pool_map, local_sem.at[10]),
+        pltpu.make_async_copy(pool_scale_hbm, pool_scale, local_sem.at[11]),
+        pltpu.make_async_copy(group_router_hbm, group_router, local_sem.at[12]),
+        pltpu.make_async_copy(expert_router_hbm, expert_router, local_sem.at[13]),
     ]
-    for copy in local:
-        copy.start()
-
-    barrier = pltpu.get_barrier_semaphore()
-
-    def greet(ep_to, tp_to):
-        pl.semaphore_signal(
-            barrier, inc=1, device_id={"ep": ep_to, "tp": tp_to}, device_id_type=MESH
-        )
-
-    @pl.loop(1, n)
-    def _(d):
-        greet(((z + d) % n) * n + yc, tp)
-        greet(z * n + (yc + d) % n, tp)
-
-    greet(ep, mate)
-    greet(ep, across)
-    greet(ahead, tp)
-    greet(behind, tp)
+    for i in (0, 7, 8, 1, 2, 9, 3, 10, 11, 4, 5, 6, 12, 13):
+        local[i].start()
+
+    spans = [pl.ds(sum(BACK[:k]), BACK[k]) for k in range(len(BACK))]
+
     def gate_copy(k):
         return remote(
             gate_hbm.at[0, cols(k)], gate.at[1, cols(k)], ws.at[0, k], wr.at[0, k], ep, mate
@@ -192,10 +210,10 @@
 
     def down_copy(k):
         return remote(
-            down_hbm.at[0, :, cols(k)],
-            down.at[1, :, cols(k)],
-            ws.at[2, k],
-            wr.at[2, k],
+            down_hbm.at[0, :, spans[k]],
+            down.at[1, :, spans[k]],
+            ds.at[k],
+            dr.at[k],
             ep,
             mate,
         )
@@ -209,9 +227,9 @@
         return remote(src.at[part(to), at], dst.at[part(z), at], send, recv.at[k], to * n + yc, tp)
 
     def start_all(copy, *args):
-        @pl.loop(1, n)
-        def _(d):
-            copy(*args, d).start()
+        @pl.loop(0, n - 1)
+        def _(i):
+            copy(*args, n // 2 + (i + 1) // 2 * (1 - 2 * (i % 2))).start()
 
     others = pl.ds(0, slots - block)
 
@@ -229,6 +247,8 @@
     y_back = (y_copy, ysend2, ybuf2, ys2, yr2)
 
     local[0].wait()
+    local[7].wait()
+    local[8].wait()
     normed[...] = norm_rows(xin[...], exp_gain[...])
     everyone = routes.shape[1]
     named = routes[...].astype(F32)
@@ -263,15 +283,16 @@
 
     local[1].wait()
     local[2].wait()
+    local[9].wait()
     total = mix_in.shape[0]
     step = 128
 
-    @pl.loop(0, total // step)
-    def _(b):
+    def pool_rows(b):
         at = pl.multiple_of(b * step, step)
         good = norm_rows(mix_in[pl.ds(at, step), :], mix_gain[...])
         pin[pl.ds(at + step, step), :] = dot(good, pool_in[...]).astype(BF16)
 
+    pool_rows(total // step - 1)
     border_copy = remote(
         pin.at[pl.ds(total + step - RIM, RIM)], border, ms.at[0], mr.at[0], ahead, tp
     )
@@ -280,18 +301,22 @@
         pl.semaphore_wait(barrier, 2 * (n - 1) + 4)
     border_copy.start()
 
+    gate_copy(0).start()
+    up_copy(0).start()
     for k in range(Z_FIRST):
         start_all(*z_early, k, cols(k))
     for k in range(Z_FIRST, Z_FIRST + 3):
         start_all(*y_out, k, cols(k))
 
-    @pl.loop(0, CHUNKS)
+    @pl.loop(1, CHUNKS - 1)
     def _(k):
         gate_copy(k).start()
         up_copy(k).start()
 
-    @pl.loop(0, CHUNKS)
-    def _(k):
+    down_copy(0).start()
+    gate_copy(CHUNKS - 1).start()
+    up_copy(CHUNKS - 1).start()
+    for k in range(1, len(BACK)):
         down_copy(k).start()
 
     ybuf[part(z), early] = zsend[part(z), early]
@@ -339,6 +364,7 @@
             part_copy(k, d).start()
 
 
+    pl.loop(0, total // step - 1)(pool_rows)
     with scope("wait_border"):
         border_copy.wait_recv()
     pin[pl.ds(0, step - RIM), :] = jnp.zeros((step - RIM, pin.shape[1]), BF16)
@@ -348,6 +374,8 @@
     back = iota((step, 2 * step), 0) + step - iota((step, 2 * step), 1)
     band = ones_where((back >= 0) & (back < window))
     local[3].wait()
+    local[10].wait()
+    local[11].wait()
 
     @pl.loop(0, total // step)
     def _(b):
@@ -433,25 +461,26 @@
     arrive_late(0)
     to_z(Z_FIRST + 3)
     arrive_late(1)
+    arrive(Z_FIRST)
     to_z(Z_FIRST + 4)
-    arrive(Z_FIRST)
+    arrive(Z_FIRST + 1)
     to_z(Z_FIRST + 5)
 
     gsum[...] = jnp.zeros_like(gsum)
     usum[...] = jnp.zeros_like(usum)
-    for copy in local[4:]:
-        copy.wait()
+    for i in (4, 5, 6, 12, 13):
+        local[i].wait()
 
     def accumulate(r, w, k):
         x = rows[r, :, cols(k)]
         gsum[r, w] += dot(x, gate[w, cols(k), :])
         usum[r, w] += dot(x, up[w, cols(k), :])
 
-    @pl.loop(0, Z_FIRST + 1)
+    @pl.loop(0, Z_FIRST + 2)
     def _(k):
         accumulate(0, 0, k)
 
-    @pl.loop(Z_FIRST + 1, CHUNKS)
+    @pl.loop(Z_FIRST + 2, CHUNKS)
     def _(k):
         arrive(k)
         accumulate(0, 0, k)
@@ -486,25 +515,27 @@
     weight0 = picked0 / (picked0 + picked1)
     weight1 = picked1 / (picked0 + picked1)
 
-    @pl.loop(0, CHUNKS)
-    def _(k):
+    def wait_weights(k):
         with scope("wait_w"):
             gate_copy(k).wait_recv()
             up_copy(k).wait_recv()
-        accumulate(0, 1, k)
+
+    def wait_rows(k):
         with scope("wait_r"):
             row_copy(k).wait_recv()
+
+    @pl.loop(0, CHUNKS - 1)
+    def _(k):
+        wait_weights(k)
+        accumulate(0, 1, k)
+        wait_rows(k)
         accumulate(1, 0, k)
         accumulate(1, 1, k)
 
-    @pl.loop(0, 2)
-    def _(r):
+    def activate(r):
         @pl.loop(0, 2)
         def _(w):
-            g = gsum[r, w]
-            hidden[r, w] = (jax.nn.silu(g) * usum[r, w]).astype(BF16)
-
-    spans = [pl.ds(sum(BACK[:k]), BACK[k]) for k in range(len(BACK))]
+            hidden[r, w] = (jax.nn.silu(gsum[r, w]) * usum[r, w]).astype(BF16)
 
     def partial_copy(k):
         at = spans[k]
@@ -515,11 +546,13 @@
 
     def down_stage(k):
         at = spans[k]
-        if at.start % width == 0:
-            with scope("wait_down"):
-                down_copy(at.start // width).wait_recv()
+        with scope("wait_down"):
+            down_copy(k).wait_recv()
         psend[:, at] = project(1, at).astype(BF16)
         partial_copy(k).start()
+        if k == 0:
+            accumulate(0, 1, CHUNKS - 1)
+            activate(0)
         pown[:, at] = project(0, at)
 
     def z_stage(k):
@@ -550,6 +583,12 @@
         exp_fin[:, at] = (weight0 * both[:tokens] + weight1 * both[tokens:]).astype(BF16)
         exp_copy(k).start()
 
+    last = CHUNKS - 1
+    wait_rows(last)
+    accumulate(1, 0, last)
+    wait_weights(last)
+    accumulate(1, 1, last)
+    activate(1)
     stages = ((down_stage, 0), (z_stage, 2), (y_stage, 4), (finish, 6))
     for turn in range(len(BACK) + 6):
         for stage, later in stages:
@@ -558,32 +597,38 @@
                     stage(turn - later)
         if 0 <= turn - len(BACK) + 1 < PIECES - ACROSS_FIRST:
             mix_stage(turn - len(BACK) + 1 + ACROSS_FIRST)
-    for j in range(PIECES):
-        mix_finish(j)
+        if turn == 1:
+            border_copy.wait_send()
+            sent_all(ysend, ys)
+            sent_all(zsend, zs)
+
+            @pl.loop(0, CHUNKS)
+            def _(k):
+                gate_copy(k).wait_send()
+                up_copy(k).wait_send()
+                row_copy(k).wait_send()
+
+        if turn == len(BACK) + 3:
+            for j in range(PIECES - 1):
+                mix_finish(j)
+    mix_finish(PIECES - 1)
 
     with scope("sent"):
-        border_copy.wait_send()
-        for src, send in ((ysend, ys), (zsend, zs), (ysend2, ys2), (zsend2, zs2)):
-            sent_all(src, send)
-
-    for j in range(PIECES):
-        mix_copy1(j, 0).wait_send()
-        mix_copy1(j, 1).wait_send()
-        mix_copy2(j).wait_send()
-
-    @pl.loop(0, CHUNKS)
-    def _(k):
-        gate_copy(k).wait_send()
-        up_copy(k).wait_send()
-        down_copy(k).wait_send()
-        row_copy(k).wait_send()
-
-    for k in range(len(BACK)):
-        partial_copy(k).wait_send()
-        exp_copy(k).wait()
-
-    for j in range(PIECES):
-        mix_out_copy(j).wait()
+        sent_all(zsend2, zs2)
+        sent_all(ysend2, ys2)
+
+        for j in range(PIECES):
+            mix_copy1(j, 0).wait_send()
+            mix_copy1(j, 1).wait_send()
+            mix_copy2(j).wait_send()
+
+        for k in range(len(BACK)):
+            down_copy(k).wait_send()
+            partial_copy(k).wait_send()
+            exp_copy(k).wait()
+
+        for j in range(PIECES):
+            mix_out_copy(j).wait()
 
 
 def write_out(mix_from, exp_from, mix_to, exp_to, mix_held, exp_held, in_sem, out_sem):
@@ -632,7 +677,6 @@
     cap = 4 * tokens // experts
     slots = cap * experts
     hid = gate_weight.shape[2]
-    vmem = pl.BlockSpec(memory_space=pltpu.VMEM)
     hbm = pl.BlockSpec(memory_space=pl.ANY)
     dma = pltpu.SemaphoreType.DMA
     each, back = dma((CHUNKS,)), dma((len(BACK),))
@@ -642,7 +686,7 @@
             jax.ShapeDtypeStruct((total // 4, model), BF16),
             jax.ShapeDtypeStruct((tokens, model), BF16),
         ),
-        in_specs=[hbm, vmem, hbm, vmem, vmem, hbm, hbm, vmem, vmem, vmem, vmem, hbm, hbm, hbm],
+        in_specs=[hbm] * 14,
         out_specs=(hbm, hbm),
         scratch_shapes=[
             pltpu.VMEM((total, model), BF16),
@@ -676,7 +720,7 @@
             pltpu.VMEM((slots, model), BF16),
             pltpu.VMEM((slots, model), BF16),
             pltpu.VMEM((slots, model), BF16),
-            dma((7,)),
+            dma((14,)),
             dma,
             each,
             dma,
@@ -689,8 +733,8 @@
             each,
             back,
             back,
-            dma((3, CHUNKS)),
-            dma((3, CHUNKS)),
+            dma((2, CHUNKS)),
+            dma((2, CHUNKS)),
             dma((1,)),
             dma((1,)),
             dma((PIECES, 2)),
@@ -702,6 +746,15 @@
             pltpu.VMEM((total // 4, model), BF16),
             dma((len(BACK),)),
             dma((PIECES,)),
+            back,
+            back,
+            pltpu.VMEM((model,), BF16),
+            pltpu.VMEM((1, channels, channels), BF16),
+            pltpu.VMEM((channels,), BF16),
+            pltpu.VMEM((model,), BF16),
+            pltpu.VMEM((group_router.shape[1], model), BF16),
+            pltpu.VMEM((experts, model), BF16),
+            pltpu.VMEM((2, 4 * tokens), jnp.int32),
         ],
         compiler_params=pltpu.CompilerParams(
             collective_id=0, has_side_effects=True, vmem_limit_bytes=60 * 1024 * 1024

time: 117 us -> 112 us (0.957)
  Pallas kernels: 116 us -> 111 us
    pallas_call x1, Pallas kernels: 114 us -> 109 us  [on_device(): pl.pallas_call(functools.partial(kernel, n, cap), out_shape=(jax.ShapeDty...]
where the time goes in v3:
time: 112 us
  Pallas kernels  111 us (99%)
    pallas_call x1, Pallas kernels, on_device(): pl.pallas_call(functools.partial(kernel, n, cap), out_shape=(jax.ShapeDty...  109 us

profile of v3, /device:TPU:1, one launch (start us, length us, event | category | flops | bytes accessed | tf_op | source)
XLA Modules:
  0.0 111.9 jit_solution(9471645232670266214)
XLA Ops:
  0.6 109.2 %shard_map.149 = (bf16[128,2048]{1,0:T(8,128)(2,1)}, bf16[96,2048]{1,0:T(8,128)(2,1)}) custom-call(bf16[512,2048]{1,0:T(8,128)(2,1)} %mix_hbm.1, bf16[2048]{0:T(1024)(128)(2,1)} %mix_gain_hbm.1, bf16[2048,256]{1,0:T(8,128)(2,1)} %pool_in_hbm.1, bf16[1,256,256]{2,1,0:T(8,128)(2,1)} %pool_map_hbm.1, bf16[256]{0:T(256)(128)(2,1)} %pool_scale_hbm.1, ...), custom_call_target="tpu_custom_call" | custom-call | tf_op jit(solution)/shard_map/pallas_call | solution.py:683
  109.8 1.9 %shard_map.150 = (bf16[128,2048]{1,0:T(8,128)(2,1)}, bf16[96,2048]{1,0:T(8,128)(2,1)}) custom-call(bf16[128,2048]{1,0:T(8,128)(2,1)} %get-tuple-element.4.mix_from, bf16[96,2048]{1,0:T(8,128)(2,1)} %get-tuple-element.5.exp_from), custom_call_target="tpu_custom_call" | custom-call | bytes 1835008 | tf_op jit(solution)/shard_map/pallas_call | solution.py:779

commit v4 on v3

--- a/solution.py
+++ b/solution.py
@@ -168,10 +168,16 @@
             barrier, inc=1, device_id={"ep": ep_to, "tp": tp_to}, device_id_type=MESH
         )
 
-    @pl.loop(1, n)
-    def _(d):
-        greet(((z + d) % n) * n + yc, tp)
-        greet(z * n + (yc + d) % n, tp)
+    def turned(i):
+        return n // 2 + (i + 1) // 2 * (1 - 2 * (i % 2))
+
+    @pl.loop(0, n - 1)
+    def _(i):
+        greet(((z + turned(i)) % n) * n + yc, tp)
+
+    @pl.loop(0, n - 1)
+    def _(i):
+        greet(z * n + (yc + turned(i)) % n, tp)
 
     greet(ep, mate)
     greet(ep, across)
@@ -229,7 +235,7 @@
     def start_all(copy, *args):
         @pl.loop(0, n - 1)
         def _(i):
-            copy(*args, n // 2 + (i + 1) // 2 * (1 - 2 * (i % 2))).start()
+            copy(*args, turned(i)).start()
 
     others = pl.ds(0, slots - block)
 
@@ -539,7 +545,19 @@
 
     def partial_copy(k):
         at = spans[k]
-        return remote(psend.at[:, at], precv.at[:, at], ps.at[k], pr.at[k], ep, across)
+        return remote(psend.at[:, at], precv.at[:, at], ps.at[k], pr.at[k, 0], ep, across)
+
+
+    def block_copy(k, d):
+        at, rows_at = spans[k], part((z + d) % n)
+        return remote(
+            psend.at[rows_at, at],
+            precv.at[rows_at, at],
+            ps.at[k],
+            pr.at[k, d],
+            ep,
+            across,
+        )
 
     def project(r, at):
         return dot(hidden[r, 0], down[0, :, at]) + dot(hidden[r, 1], down[1, :, at])
@@ -549,7 +567,12 @@
         with scope("wait_down"):
             down_copy(k).wait_recv()
         psend[:, at] = project(1, at).astype(BF16)
-        partial_copy(k).start()
+
+        @pl.loop(0, n - 1)
+        def _(i):
+            block_copy(k, turned(i)).start()
+
+        block_copy(k, 0).start()
         if k == 0:
             accumulate(0, 1, CHUNKS - 1)
             activate(0)
@@ -557,11 +580,21 @@
 
     def z_stage(k):
         at = spans[k]
-        with scope("wait_part"):
-            partial_copy(k).wait_recv()
-        zsend2[:, at] = (pown[:, at] + precv[:, at].astype(F32)).astype(BF16)
-        start_all(*z_back, k, at)
-        zbuf2[part(z), at] = zsend2[part(z), at]
+
+        def add(rows_at):
+            return (pown[rows_at, at] + precv[rows_at, at].astype(F32)).astype(BF16)
+
+        @pl.loop(0, n - 1)
+        def _(i):
+            d = turned(i)
+            with scope("wait_part"):
+                block_copy(k, d).wait_recv()
+            rows_at = part((z + d) % n)
+            zsend2[rows_at, at] = add(rows_at)
+            z_copy(*z_back[1:], k, at, d).start()
+
+        block_copy(k, 0).wait_recv()
+        zbuf2[part(z), at] = add(part(z))
 
     def y_stage(k):
         at = spans[k]
@@ -732,7 +765,7 @@
             each,
             each,
             back,
-            back,
+            dma((len(BACK), n)),
             dma((2, CHUNKS)),
             dma((2, CHUNKS)),
             dma((1,)),

time: 112 us -> 111 us (level)
  no operation moved by 1% of the time
where the time goes in v4:
time: 111 us
  Pallas kernels  110 us (99%)
    pallas_call x1, Pallas kernels, on_device(): pl.pallas_call(functools.partial(kernel, n, cap), out_shape=(jax.ShapeDty...  108 us

profile of v4, /device:TPU:1, one launch (start us, length us, event | category | flops | bytes accessed | tf_op | source)
XLA Modules:
  0.0 111.1 jit_solution(14897365258746588643)
XLA Ops:
  0.6 108.3 %shard_map.149 = (bf16[128,2048]{1,0:T(8,128)(2,1)}, bf16[96,2048]{1,0:T(8,128)(2,1)}) custom-call(bf16[512,2048]{1,0:T(8,128)(2,1)} %mix_hbm.1, bf16[2048]{0:T(1024)(128)(2,1)} %mix_gain_hbm.1, bf16[2048,256]{1,0:T(8,128)(2,1)} %pool_in_hbm.1, bf16[1,256,256]{2,1,0:T(8,128)(2,1)} %pool_map_hbm.1, bf16[256]{0:T(256)(128)(2,1)} %pool_scale_hbm.1, ...), custom_call_target="tpu_custom_call" | custom-call | tf_op jit(solution)/shard_map/pallas_call | solution.py:716
  109.0 1.9 %shard_map.150 = (bf16[128,2048]{1,0:T(8,128)(2,1)}, bf16[96,2048]{1,0:T(8,128)(2,1)}) custom-call(bf16[128,2048]{1,0:T(8,128)(2,1)} %get-tuple-element.4.mix_from, bf16[96,2048]{1,0:T(8,128)(2,1)} %get-tuple-element.5.exp_from), custom_call_target="tpu_custom_call" | custom-call | bytes 1835008 | tf_op jit(solution)/shard_map/pallas_call | solution.py:812

commit v5 on v4

--- a/solution.py
+++ b/solution.py
@@ -664,26 +664,15 @@
             mix_out_copy(j).wait()
 
 
-def write_out(mix_from, exp_from, mix_to, exp_to, mix_held, exp_held, in_sem, out_sem):
-    whole = ((mix_from, mix_held, mix_to), (exp_from, exp_held, exp_to))
-
-    def copies(i, h):
-        source, held, target = whole[i]
-        size = held.shape[0] // 2
-        at = pl.ds(h * size, size)
-        return (
-            pltpu.make_async_copy(source.at[at], held.at[at], in_sem.at[i, h]),
-            pltpu.make_async_copy(held.at[at], target.at[at], out_sem.at[i, h]),
-        )
-
-    each = [copies(i, h) for i in range(2) for h in range(2)]
-    for copy_in, _ in each:
-        copy_in.start()
-    for copy_in, copy_out in each:
-        copy_in.wait()
-        copy_out.start()
-    for _, copy_out in each:
-        copy_out.wait()
+def write_out(mix_from, exp_from, mix_to, exp_to, sem):
+    copies = (
+        pltpu.make_async_copy(mix_from, mix_to, sem.at[0]),
+        pltpu.make_async_copy(exp_from, exp_to, sem.at[1]),
+    )
+    for copy in copies:
+        copy.start()
+    for copy in copies:
+        copy.wait()
 
 
 def on_device(n, *args):
@@ -790,23 +779,28 @@
             pltpu.VMEM((2, 4 * tokens), jnp.int32),
         ],
         compiler_params=pltpu.CompilerParams(
-            collective_id=0, has_side_effects=True, vmem_limit_bytes=60 * 1024 * 1024
+            collective_id=0, has_side_effects=True, vmem_limit_bytes=53504 * 1024
         ),
     )(
-        mixer_input,
-        mixer_gain,
-        pool_in,
-        pool_map,
-        pool_scale,
-        pool_out,
-        expert_input,
-        expert_gain,
-        group_router.T,
-        expert_router.T,
-        routes.T,
-        gate_weight,
-        up_weight,
-        down_weight,
+        *(
+            pltpu.with_memory_space_constraint(value, pltpu.HBM)
+            for value in (
+                mixer_input,
+                mixer_gain,
+                pool_in,
+                pool_map,
+                pool_scale,
+                pool_out,
+                expert_input,
+                expert_gain,
+                group_router.T,
+                expert_router.T,
+                routes.T,
+                gate_weight,
+                up_weight,
+                down_weight,
+            )
+        )
     )
     shapes = [(total // 4, model), (tokens, model)]
     return pl.pallas_call(
@@ -814,7 +808,8 @@
         out_shape=tuple(jax.ShapeDtypeStruct(shape, BF16) for shape in shapes),
         in_specs=[hbm, hbm],
         out_specs=(hbm, hbm),
-        scratch_shapes=[pltpu.VMEM(shape, BF16) for shape in shapes] + [dma((2, 2)), dma((2, 2))],
+        scratch_shapes=[dma((2,))],
+        compiler_params=pltpu.CompilerParams(vmem_limit_bytes=1 << 20),
         cost_estimate=pl.CostEstimate(flops=0, bytes_accessed=4 * 224 * model, transcendentals=0),
     )(*sent)
 

time: 111 us -> 110 us (level)
  no operation moved by 1% of the time
where the time goes in v5:
time: 110 us
  Pallas kernels  109 us (99%)
    pallas_call x1, Pallas kernels, on_device(): pl.pallas_call(functools.partial(kernel, n, cap), out_shape=(jax.ShapeDty...  108 us

profile of v5, /device:TPU:1, one launch (start us, length us, event | category | flops | bytes accessed | tf_op | source)
XLA Modules:
  0.0 109.5 jit_solution(10705228805670013038)
XLA Ops:
  0.6 107.8 %shard_map.149 = (bf16[128,2048]{1,0:T(8,128)(2,1)S(1)}, bf16[96,2048]{1,0:T(8,128)(2,1)S(1)}) custom-call(bf16[512,2048]{1,0:T(8,128)(2,1)} %mix_hbm.1, bf16[2048]{0:T(1024)(128)(2,1)} %mix_gain_hbm.1, bf16[2048,256]{1,0:T(8,128)(2,1)} %pool_in_hbm.1, bf16[1,256,256]{2,1,0:T(8,128)(2,1)} %pool_map_hbm.1, bf16[256]{0:T(256)(128)(2,1)} %pool_scale_hbm.1, ...), custom_call_target="tpu_custom_call" | custom-call | tf_op jit(solution)/shard_map/pallas_call | solution.py:705
  108.4 0.9 shard_map.150

commit v6 on v5

--- a/solution.py
+++ b/solution.py
@@ -10,8 +10,8 @@
 EPS = 1e-06
 RIM = 16
 CHUNKS = 8
-Z_FIRST = 2
-PIECES = 4
+Z_FIRST = 1
+PIECES = 8
 ACROSS_FIRST = 1
 BACK = (128, 128) + (256,) * 6 + (128, 128)
 scope = jax.named_scope
@@ -454,23 +454,23 @@
 
     for j in range(ACROSS_FIRST):
         mix_project(j)
-    to_z(Z_FIRST)
-    to_z(Z_FIRST + 1)
+    to_z(1)
+    to_z(2)
     to_y(0)
-    start_all(*y_out, Z_FIRST + 3, cols(Z_FIRST + 3))
-    to_z(Z_FIRST + 2)
+    start_all(*y_out, 4, cols(4))
+    to_z(3)
     for j in range(ACROSS_FIRST, PIECES):
         mix_project(j)
-    to_y(1)
-    for k in range(Z_FIRST + 4, CHUNKS):
+    arrive_late(0)
+    for k in range(5, CHUNKS):
         start_all(*y_out, k, cols(k))
-    arrive_late(0)
-    to_z(Z_FIRST + 3)
-    arrive_late(1)
-    arrive(Z_FIRST)
-    to_z(Z_FIRST + 4)
-    arrive(Z_FIRST + 1)
-    to_z(Z_FIRST + 5)
+    arrive(1)
+    to_z(4)
+    arrive(2)
+    to_z(5)
+    arrive(3)
+    to_z(6)
+    to_z(7)
 
     gsum[...] = jnp.zeros_like(gsum)
     usum[...] = jnp.zeros_like(usum)
@@ -482,11 +482,11 @@
         gsum[r, w] += dot(x, gate[w, cols(k), :])
         usum[r, w] += dot(x, up[w, cols(k), :])
 
-    @pl.loop(0, Z_FIRST + 2)
+    @pl.loop(0, 4)
     def _(k):
         accumulate(0, 0, k)
 
-    @pl.loop(Z_FIRST + 2, CHUNKS)
+    @pl.loop(4, CHUNKS)
     def _(k):
         arrive(k)
         accumulate(0, 0, k)
@@ -628,8 +628,10 @@
             if 0 <= turn - later < len(BACK):
                 with scope(stage.__name__):
                     stage(turn - later)
-        if 0 <= turn - len(BACK) + 1 < PIECES - ACROSS_FIRST:
-            mix_stage(turn - len(BACK) + 1 + ACROSS_FIRST)
+        if turn >= len(BACK) - 1:
+            staged = ACROSS_FIRST + 2 * (turn - len(BACK) + 1)
+            for j in range(staged, min(staged + 2, PIECES)):
+                mix_stage(j)
         if turn == 1:
             border_copy.wait_send()
             sent_all(ysend, ys)
@@ -642,9 +644,10 @@
                 row_copy(k).wait_send()
 
         if turn == len(BACK) + 3:
-            for j in range(PIECES - 1):
+            for j in range(PIECES // 2):
                 mix_finish(j)
-    mix_finish(PIECES - 1)
+    for j in range(PIECES // 2, PIECES):
+        mix_finish(j)
 
     with scope("sent"):
         sent_all(zsend2, zs2)

time: 110 us -> 110 us (level)
  no operation moved by 1% of the time
where the time goes in v6:
time: 110 us
  Pallas kernels  109 us (99%)
    pallas_call x1, Pallas kernels, on_device(): pl.pallas_call(functools.partial(kernel, n, cap), out_shape=(jax.ShapeDty...  108 us

profile of v6, /device:TPU:1, one launch (start us, length us, event | category | flops | bytes accessed | tf_op | source)
XLA Modules:
  0.0 109.9 jit_solution(17704701424768519292)
XLA Ops:
  0.6 108.1 %shard_map.149 = (bf16[128,2048]{1,0:T(8,128)(2,1)S(1)}, bf16[96,2048]{1,0:T(8,128)(2,1)S(1)}) custom-call(bf16[512,2048]{1,0:T(8,128)(2,1)} %mix_hbm.1, bf16[2048]{0:T(1024)(128)(2,1)} %mix_gain_hbm.1, bf16[2048,256]{1,0:T(8,128)(2,1)} %pool_in_hbm.1, bf16[1,256,256]{2,1,0:T(8,128)(2,1)} %pool_map_hbm.1, bf16[256]{0:T(256)(128)(2,1)} %pool_scale_hbm.1, ...), custom_call_target="tpu_custom_call" | custom-call | tf_op jit(solution)/shard_map/pallas_call | solution.py:708
  108.8 0.9 shard_map.150
